TPU v7x, 512 devices: a whole 4x8x8 slice. The times are simulated.
512 devices in a mesh: sp: 128 (over z, y, core), tp: 4 (over x).
Axes of the slice: x: 4, y: 8, z: 8, core: 2. Of those that a mesh axis runs over, the one named last changes fastest.
Arguments:
- tokens: bfloat16 [65536, 2048], P(('sp', 'tp')), may hold values from -6 to 6
- norm_gain: bfloat16 [2048], replicated, may hold values from 0.099609375 to 1.8984375
- proj_x: bfloat16 [2048, 2048], P('sp', 'tp'), may hold values from -0.125 to 0.125
- gate_projection: bfloat16 [2048, 2048], P('sp', 'tp'), may hold values from -0.125 to 0.125
- conv_taps: bfloat16 [4, 2048], P(None, 'tp'), may hold values from -3 to 3
- gate_recur: bfloat16 [8, 256, 256], P('tp'), may hold values from -0.375 to 0.375
- gate_input: bfloat16 [8, 256, 256], P('tp'), may hold values from -0.375 to 0.375
- decay_param: float32 [2048], P('tp'), may hold values from 4 to 25
- decay_shift: float32 [8, 65536], P('tp', 'sp'), may hold values from -1.3 to 0, as said below
- proj_out: bfloat16 [2048, 2048], P('tp', 'sp'), may hold values from -0.125 to 0.125
Outputs:
- mixed_out: bfloat16 [65536, 2048], P(('sp', 'tp'))
Inputs may be any that keep to these rules, and one draw needn't show every extreme that they name: `decay_shift`: added log-decays, never positive.
All inputs are finite; a program needn't handle non-finite values.
Results may differ from a plain program's by a relative error of at most 0.015.
Values may be sent and summed in bfloat16 or wider, within the bound.
A program may use at most 128 MiB of HBM per device.

v0:
```python
import jax
import jax.numpy as jnp
from jax import lax
from jax.sharding import Mesh
from jax.sharding import PartitionSpec as P

HEAD = 256
CONV = 4
SP = ("sp_0", "sp_1", "sp_2")
SP_TP = ("sp_0", "sp_1", "sp_2", "tp")


def in_one_piece(arrays, axis, dim, along):
    widths = [a.shape[along] for a in arrays]
    both = jnp.concatenate(arrays, axis=along)
    out = lax.all_gather(both, axis, axis=dim, tiled=True)
    return tuple(jnp.split(out, [sum(widths[:k]) for k in range(1, len(widths))], axis=along))


def copy_for_each(array, axis):
    copies = jnp.broadcast_to(array, (lax.axis_size(axis), *array.shape))
    return lax.all_to_all(copies, axis, split_axis=0, concat_axis=0, tiled=True)


def joined_along(tiles, dim):
    tiles = jnp.moveaxis(tiles, 0, dim)
    shape = tiles.shape
    return tiles.reshape(*shape[:dim], shape[dim] * shape[dim + 1], *shape[dim + 2 :])


def gathered_copies(array, axis, dim):
    tiles = copy_for_each(array, axis)
    return joined_along(tiles, dim)


def shifted(block, axis, distance):
    devices = range(lax.axis_size(axis))
    route = [(i - distance, i) for i in devices if i - distance in devices]
    return lax.ppermute(block, axis, route)


def nothing_yet(array, identity):
    return jax.tree.map(
        lambda a, e: jnp.broadcast_to(jnp.asarray(e, a.dtype), a.shape), array, identity
    )


def all_in_one(array, axis):
    leaves = jax.tree.leaves(array)
    order = sorted(range(len(leaves)), key=lambda k: -leaves[k].size)
    width = (1, *leaves[order[0]].shape)[-1]
    lines = [
        jnp.pad(leaves[k].reshape(-1), (0, -leaves[k].size % width)).reshape(-1, width)
        for k in order
    ]
    both, at, found = (lax.all_gather(jnp.concatenate(lines), axis), 0, {})
    for k, line in zip(order, lines):
        share = both[:, at : at + len(line)].reshape(len(both), -1)
        found[k] = share[:, : leaves[k].size].reshape(-1, *leaves[k].shape)
        at += len(line)
    numbers = iter(range(len(leaves)))
    return jax.tree.map(lambda _: found[next(numbers)], array)


def entering(array, axes, combine, identity):
    before = start = nothing_yet(array, identity)
    subtotal = array
    for axis in reversed(axes):
        size, index = (lax.axis_size(axis), lax.axis_index(axis))
        pieces = all_in_one(subtotal, axis)
        inside, subtotal = (start, start)
        for k in range(size):
            passed = k < index
            subtotal = combine(subtotal, jax.tree.map(lambda part: part[k], pieces))
            inside = jax.tree.map(lambda new, old: jnp.where(passed, new, old), subtotal, inside)
        before = combine(inside, before)
    return before


def in_blocks(array, dim, size):
    shape = array.shape
    tiles = array.reshape(*shape[:dim], size, shape[dim] // size, *shape[dim + 1 :])
    return jnp.moveaxis(tiles, dim, 0)


def summed_on_arrival(array, axis, dim):
    tiles = in_blocks(array, dim, lax.axis_size(axis))
    arrived = lax.all_to_all(tiles, axis, split_axis=0, concat_axis=0, tiled=True)
    return arrived.astype(jnp.float32).sum(axis=0)


def rms_norm(values, norm_gain):
    floats = values.astype(jnp.float32)
    scaled = floats * lax.rsqrt(jnp.mean(floats * floats, axis=-1, keepdims=True) + 1e-06)
    return (scaled * norm_gain.astype(jnp.float32)).astype(jnp.bfloat16)


def combine_pair(earlier, later):
    return (earlier[0] * later[0], later[0] * earlier[1] + later[1])


def on_device(
    tokens,
    norm_gain,
    proj_x,
    gate_projection,
    conv_taps,
    gate_recur,
    gate_input,
    decay_param,
    decay_shift,
    proj_out,
):
    normed = rms_norm(tokens, norm_gain)
    full_x, full_gate = in_one_piece((proj_x, gate_projection), SP, 0, 1)
    local_width = proj_x.shape[1]
    piece = gathered_copies(normed, "tp", 0)
    branch_piece = jnp.dot(piece, full_x, preferred_element_type=jnp.float32).astype(jnp.bfloat16)
    gating_piece = jnp.dot(piece, full_gate, preferred_element_type=jnp.float32).astype(
        jnp.bfloat16
    )
    joined = jnp.concatenate([branch_piece, gating_piece], axis=1)
    branch = joined[:, :local_width]
    gating = joined[:, local_width:]
    row_count = branch.shape[0]
    tail_rows = shifted(branch[row_count - CONV + 1 :], SP, 1)
    extended = jnp.concatenate([tail_rows, branch], axis=0)
    conv_sum = jnp.zeros((row_count, local_width), jnp.float32)
    for tap_index in range(CONV):
        conv_sum = conv_sum + extended[tap_index : tap_index + row_count].astype(
            jnp.float32
        ) * conv_taps[tap_index].astype(jnp.float32)
    conved = conv_sum.astype(jnp.bfloat16)
    head_count = gate_recur.shape[0]
    grouped = conved.reshape(row_count, head_count, HEAD)
    recur = jax.nn.sigmoid(
        jnp.einsum("thi,hij->thj", grouped, gate_recur, preferred_element_type=jnp.float32)
    )
    inlet = jax.nn.sigmoid(
        jnp.einsum("thi,hij->thj", grouped, gate_input, preferred_element_type=jnp.float32)
    )
    decay_rate = jax.nn.softplus(-decay_param).reshape(head_count, HEAD)
    log_decay = (-8.0 * recur * decay_rate[None] + jnp.transpose(decay_shift)[:, :, None]).reshape(
        row_count, local_width
    )
    decay = jnp.exp(log_decay)
    drive = (
        jnp.sqrt(-jnp.expm1(2.0 * log_decay))
        * inlet.reshape(row_count, local_width)
        * conved.astype(jnp.float32)
    )
    identity = (jnp.ones((local_width,), jnp.float32), jnp.zeros((local_width,), jnp.float32))
    cumulative, local_state = lax.associative_scan(combine_pair, (decay, drive), axis=0)
    carried = entering(
        (cumulative[row_count - 1], local_state[row_count - 1]), SP, combine_pair, identity
    )
    states = local_state + cumulative * carried[1][None, :]
    mixed = (states * jax.nn.gelu(gating.astype(jnp.float32))).astype(jnp.bfloat16)
    out_cols = lax.all_gather(proj_out, SP, axis=1, tiled=True)
    summed_out = summed_on_arrival(
        jnp.dot(mixed, out_cols, preferred_element_type=jnp.float32).astype(jnp.bfloat16), "tp", 0
    )
    return summed_out.astype(jnp.bfloat16)


def solution(mesh):
    split = Mesh(mesh.devices.reshape(8, 8, 2, mesh.shape["tp"]), ("sp_0", "sp_1", "sp_2", "tp"))
    in_specs = (
        P(SP_TP, None),
        P(),
        P(SP, "tp"),
        P(SP, "tp"),
        P(None, "tp"),
        P("tp", None, None),
        P("tp", None, None),
        P("tp"),
        P("tp", SP),
        P("tp", SP),
    )
    out_specs = P(SP_TP, None)
    return jax.shard_map(
        on_device, mesh=split, in_specs=in_specs, out_specs=out_specs, check_vma=False
    )
```

profile of v0, /device:TPU:2, one launch (start us, length us, event | category | flops | bytes accessed | tf_op | source)
XLA Modules:
  0.0 292.5 jit_solution(13550174995697596662)
XLA Ops:
  6.5 1.4 pad_maximum_fusion.9
  8.0 0.7 convert_element_type.53
  8.7 1.2 fusion.21
  9.9 1.2 fusion.23
  11.1 1.7 broadcast_in_dim.4
  12.8 9.6 %all-to-all-start = ((bf16[4,128,2048]{2,1,0:T(8,128)(2,1)}), bf16[4,128,2048]{2,1,0:T(8,128)(2,1)S(1)}, u32[]{:S(2)}, u32[]{:S(2)}) async-start(bf16[4,128,2048]{2,1,0:T(8,128)(2,1)} %broadcast_in_dim.4), calls=%async_computation | async-start | bytes 4194304 | tf_op jit(solution)/shard_map/all_to_all | solution.py:22
  22.4 0.7 all-gather.11.cloned.1.call-update
  23.2 19.5 %all-to-all-done = bf16[4,128,2048]{2,1,0:T(8,128)(2,1)S(1)} async-done(((bf16[4,128,2048]{2,1,0:T(8,128)(2,1)}), bf16[4,128,2048]{2,1,0:T(8,128)(2,1)S(1)}, u32[]{:S(2)}, u32[]{:S(2)}) %all-to-all-start) | async-done | bytes 2097184 | tf_op jit(solution)/shard_map/all_to_all | solution.py:22
  42.6 56.9 %all-gather.9.cloned.1.call-done = bf16[2048,1024]{1,0:T(8,128)(2,1)} async-done(((bf16[16,1024]{1,0:T(8,128)(2,1)}), bf16[2048,1024]{1,0:T(8,128)(2,1)}) %all-gather.9.cloned.1.call-update) | async-done | bytes 4194320 | tf_op jit(solution)/shard_map/all_gather | solution.py:16
  99.6 2.8 fusion.15
  102.4 2.1 collective-permute-start
  104.7 0.7 collective-permute-done
  105.4 0.5 add_convert_fusion
  105.9 0.6 fusion.77
  106.7 0.4 copy-done.12
  107.1 1.9 fusion.8
  109.0 1.6 copy.31
  110.5 1.2 convert_multiply_fusion.5
  111.7 2.3 slice.553
  114.1 2.1 slice.491
  116.1 2.1 slice.490
  118.4 19.5 %slice.489 = f32[256,512]{0,1:T(8,128)S(1)} slice(f32[512,512]{0,1:T(8,128)S(1)} %bitcast.159), slice={[1:512:2], [0:512:1]} | slice | bytes 1048576 | tf_op jit(solution)/shard_map/slice | solution.py:153
  137.9 19.4 %slice.488 = f32[255,512]{0,1:T(8,128)S(1)} slice(f32[512,512]{0,1:T(8,128)S(1)} %bitcast.160), slice={[2:512:2], [0:512:1]} | slice | bytes 1044480 | tf_op jit(solution)/shard_map/slice | solution.py:153
  157.3 19.5 %slice.493 = f32[256,512]{0,1:T(8,128)S(1)} slice(f32[512,512]{0,1:T(8,128)S(1)} %bitcast.161), slice={[0:511:2], [0:512:1]} | slice | bytes 1048576 | tf_op jit(solution)/shard_map/slice | solution.py:153
  176.7 1.0 copy.34
  178.1 1.3 multiply_add_fusion
  179.4 0.3 slice.551
  179.7 0.3 slice.497
  180.1 0.3 slice.496
  180.4 0.3 slice.499
  180.7 0.3 slice.495
  181.1 0.3 slice.494
  182.2 0.4 slice.500
  183.5 1.0 copy.33
  186.5 0.8 copy-done.7
  187.5 1.2 fusion.43
  188.7 2.7 pad.144
  191.5 2.7 pad.126
  194.2 2.8 pad.127
  196.9 2.8 pad.145
  199.7 0.7 slice_add_fusion.8
  200.4 0.7 slice_add_fusion.9
  201.2 2.3 all-gather.3
  203.5 27.0 %all-gather.4 = f32[8,2,512]{2,1,0:T(2,128)S(1)} all-gather(f32[1,2,512]{2,1,0:T(2,128)S(1)} %maximum_bitcast_fusion.1), channel_id=3, replica_groups=mesh['sp_0'=8,'sp_1'=8,'sp_2'=2,'tp'=4] {'sp_1'}, dimensions={0}, use_global_device_ids=true | all-gather | bytes 36864 | tf_op jit(solution)/shard_map/all_gather | solution.py:56
  230.5 26.3 %all-gather.5 = f32[8,2,512]{2,1,0:T(2,128)S(1)} all-gather(f32[1,2,512]{2,1,0:T(2,128)S(1)} %maximum_bitcast_fusion.2), channel_id=4, replica_groups=mesh['sp_0'=8,'sp_1'=8,'sp_2'=2,'tp'=4] {'sp_0'}, dimensions={0}, use_global_device_ids=true | all-gather | bytes 36864 | tf_op jit(solution)/shard_map/all_gather | solution.py:56
  256.9 7.6 %convolution_convert_fusion = bf16[512,2048]{1,0:T(8,128)(2,1)} fusion(bf16[512,2048]{0,1:T(8,128)(2,1)} %all-gather.11.cloned.1.call-done, bf16[512,2048]{1,0:T(8,128)(2,1)S(1)} %bitcast.165, bf16[2048,1024]{1,0:T(8,128)(2,1)} %all-gather.9.cloned.1.call-done, f32[512,512]{1,0:T(8,128)} %pad.144, f32[512,512]{1,0:T(8,128)} %pad.145, f32[512,512]{1,0:T(8,128)} %pad.126, ...), kind=kOutput, calls=%fused_computation | convolution fusion | flops 2152726528 | bytes 12584960 | tf_op jit(solution)/shard_map/dot_general | solution.py:161
  264.5 19.9 %all_to_all.10 = bf16[4,128,2048]{2,1,0:T(8,128)(2,1)S(1)} all-to-all(bf16[4,128,2048]{2,1,0:T(8,128)(2,1)} %bitcast.166), channel_id=1, replica_groups=mesh['sp_0'=8,'sp_1'=8,'sp_2'=2,'tp'=4] {'tp'}, dimensions={0} | all-to-all | bytes 4194304 | tf_op jit(solution)/shard_map/all_to_all | solution.py:88
  284.4 1.3 reduce_sum.22
  (169 shorter events, 4.2 us)
Async XLA Ops:
  6.5 99.4 %copy-start = (bf16[2,256,256]{2,1,0:T(8,128)(2,1)S(1)}, bf16[2,256,256]{2,1,0:T(8,128)(2,1)}, u32[]{:S(2)}) copy-start(bf16[2,256,256]{2,1,0:T(8,128)(2,1)} %param.15) | copy-start | bytes 786436
  6.5 93.0 %all-gather.9.cloned.1.call-start = ((), (), s32[]{:S(2)}) async-start(), calls=%async_computation.2 | async-start | bytes 4227072 | tf_op jit(solution)/shard_map/all_gather | solution.py:16
  12.8 10.3 %copy-start.10 = (bf16[4,512]{1,0:T(4,128)(2,1)S(1)}, bf16[4,512]{1,0:T(4,128)(2,1)}, u32[]{:S(2)}) copy-start(bf16[4,512]{1,0:T(4,128)(2,1)} %param.14) | copy-start | bytes 12292
  12.8 29.8 %all-to-all-start = ((bf16[4,128,2048]{2,1,0:T(8,128)(2,1)}), bf16[4,128,2048]{2,1,0:T(8,128)(2,1)S(1)}, u32[]{:S(2)}, u32[]{:S(2)}) async-start(bf16[4,128,2048]{2,1,0:T(8,128)(2,1)} %broadcast_in_dim.4), calls=%async_computation | async-start | bytes 4194304 | tf_op jit(solution)/shard_map/all_to_all | solution.py:22
  22.4 234.5 %all-gather.11.cloned.1.call-start = ((), (), s32[]{:S(2)}) async-start(), calls=%async_computation.3 | async-start | bytes 2113536 | tf_op jit(solution)/shard_map/all_gather | solution.py:159
  42.6 59.8 %copy-start.3 = (bf16[4,128,2048]{2,1,0:T(8,128)(2,1)}, bf16[4,128,2048]{2,1,0:T(8,128)(2,1)S(1)}, u32[]{:S(2)}) copy-start(bf16[4,128,2048]{2,1,0:T(8,128)(2,1)S(1)} %all-to-all-done) | copy-start | bytes 6291460
  99.6 5.0 %copy-start.11 = (f32[512]{0:T(512)S(1)}, f32[512]{0:T(512)}, u32[]{:S(2)}) copy-start(f32[512]{0:T(512)} %param.17) | copy-start | bytes 6148
  99.6 6.3 %copy-start.13 = (f32[2,512]{1,0:T(2,128)S(1)}, f32[2,512]{1,0:T(2,128)}, u32[]{:S(2)}) copy-start(f32[2,512]{1,0:T(2,128)} %param.18) | copy-start | bytes 12292
  102.4 2.9 %collective-permute-start = (bf16[3,512]{1,0:T(4,128)(2,1)S(1)}, bf16[3,512]{1,0:T(4,128)(2,1)S(1)}, u32[]{:S(2)}, u32[]{:S(2)}) collective-permute-start(bf16[3,512]{1,0:T(4,128)(2,1)S(1)} %slice.610), channel_id=1, source_target_pairs={{0,4},{4,8},{8,12},{12,16},{16,20},{20,24},{24,28},{28,32},{32,36}... | collective-permute-start | bytes 9224 | tf_op jit(solution)/shard_map/ppermute | solution.py:39
  105.9 0.8 copy-start.2
  105.9 1.1 copy-start.12
  111.7 26.1 %copy-start.1 = (f32[512,512]{1,0:T(8,128)}, f32[512,512]{1,0:T(8,128)S(1)}, u32[]{:S(2)}) copy-start(f32[512,512]{1,0:T(8,128)S(1)} %convert_multiply_fusion.5) | copy-start | bytes 3145732
  176.7 1.2 copy-start.5
  176.7 1.4 copy-start.6
  186.3 1.0 copy-start.7
  186.3 1.2 copy-start.8
  188.6 2.8 slice-start
  188.6 2.8 copy-start.9
  194.2 62.8 %copy-start.4 = (bf16[4,128,2048]{2,1,0:T(8,128)(2,1)S(1)}, bf16[4,128,2048]{2,1,0:T(8,128)(2,1)}, u32[]{:S(2)}) copy-start(bf16[4,128,2048]{2,1,0:T(8,128)(2,1)} %copy-done.3) | copy-start | bytes 6291460
Sparse Core Ops, SparseCore 0:
  10.5 89.0 all-gather.8
  102.7 79.8 all-gather.10
where the time goes:
time: 293 us
  local copies, waits for them, and re-layouts  87.4 us (30%)
  waiting for transfers between devices  77.9 us (27%)
  blocking collectives  75.3 us (26%)
  between operations  14.5 us (5%)
  matrix products  12.9 us (4%)
  other arithmetic  12.8 us (4%)
  starting transfers between devices  11.7 us (4%)
    slice x61, local copies, waits for them, and re-layouts, on_device(): lax.associative_scan(combine_pair, (decay, drive), axis=0)  68.6 us
    all_gather x1, waiting for transfers between devices, in_one_piece(): out = lax.all_gather(both, axis, axis=dim, tiled=True)  56.9 us
    all_gather x3, blocking collectives, all_in_one(): both, at, found = (lax.all_gather(jnp.concatenate(lines), axis), 0, {})  55.5 us
    all_to_all x1, blocking collectives, summed_on_arrival(): lax.all_to_all(tiles, axis, split_axis=0, concat_axis=0, tiled=True)  19.9 us
    all_to_all x1, waiting for transfers between devices, copy_for_each(): return lax.all_to_all(copies, axis, split_axis=0, concat_axis=0, tiled=True)  19.5 us
    pad x32, local copies, waits for them, and re-layouts, on_device(): lax.associative_scan(combine_pair, (decay, drive), axis=0)  11.6 us
    all_to_all x1, starting transfers between devices, copy_for_each(): return lax.all_to_all(copies, axis, split_axis=0, concat_axis=0, tiled=True)  9.58 us
    dot_general x1, matrix products, on_device(): jnp.dot(mixed, out_cols, preferred_element_type=jnp.float32)  7.58 us
  transfers between devices with their start and end apart: 4, of which 3 were waited for; matrix products, arithmetic and copies ran while one was open for 35% of the time, Pallas kernels for 0%

commit v1 on v0

v1 whole, which is shorter than its diff:
```python
import functools

import jax
import jax.numpy as jnp
from jax import lax
from jax.experimental import pallas as pl
from jax.experimental.pallas import tpu as pltpu
from jax.sharding import Mesh
from jax.sharding import PartitionSpec as P

HEAD = 256
CONV = 4
SP = ("sp_0", "sp_1", "sp_2")
SP_TP = ("sp_0", "sp_1", "sp_2", "tp")
MESH = pl.DeviceIdType.MESH
F32 = jnp.float32
BF16 = jnp.bfloat16
LANES = 128


def body(
    nz, ny,
    tokens, gain, proj_x, gate_proj, taps, gate_recur, gate_input, decay_param, decay_shift, proj_out,
    out,
    tok, nrm, stage, wb, gr, gi, branch, dec, drv, shiftc, gel, mx, tail,
    mine1, s1, mine2, s2, cin, dummy, outv,
    po_far, po_next, po_prev, in_rel, in_prev, in_next,
    lsem, gsem, tsend, trecv, p1send, p1recv, rsend, rrecv, dsend, drecv, xsem, osend, orecv,
):
    z, y, c, x = (lax.axis_index(a) for a in SP_TP)
    t = tok.shape[1]
    half = t // 2
    rows = 4 * t
    chunk = rows // 8
    width = 2 * wb.shape[-1]
    groups = width // LANES
    heads = width // HEAD
    pw = width // 2
    nr = wb.shape[2]
    sp_index = (z * ny + y) * 2 + c
    sp_count = nz * ny * 2

    def at(dz=0, dy=0, dc=None, dx=0, core=None):
        cc = c if dc is None else lax.rem(c + dc, 2)
        cc = cc if core is None else core
        return {
            "sp_0": lax.rem(z + dz + nz, nz), "sp_1": lax.rem(y + dy + ny, ny),
            "sp_2": cc, "tp": lax.rem(x + dx + 4, 4),
        }

    def remote(src, dst, send, recv, where):
        return pltpu.make_async_remote_copy(
            src_ref=src, dst_ref=dst, send_sem=send, recv_sem=recv, device_id=where, device_id_type=MESH
        )

    right, left = lax.rem(x + 1, 4), lax.rem(x + 3, 4)
    far = lax.rem(x + 2, 4)

    nsp = lax.rem(sp_index + 1, sp_count)
    psp = lax.rem(sp_index + sp_count - 1, sp_count)

    def of_sp(s):
        return {"sp_0": s // (2 * ny), "sp_1": lax.rem(s // 2, ny), "sp_2": lax.rem(s, 2), "tp": x}

    own_tok = pltpu.make_async_copy(tokens, tok.at[x], lsem.at[0])
    own_tok.start()
    ring = z * (1 - c) + y * c
    cross = y * (1 - c) + z * c
    core_row = pl.multiple_of(c * 16, 16)
    core_col = pl.multiple_of(c * pw, pw)
    stage_loads = []
    for m, src in enumerate((proj_x, gate_proj, proj_out)):
        loads = []
        for p in range(2):
            loads.append(pltpu.make_async_copy(src.at[:, pl.ds(p * pw, pw)], stage.at[m, p], lsem.at[1 + 3 * m + p]))
        loads.append(pltpu.make_async_copy(
            src.at[:, pl.ds(core_col, pw)], wb.at[m, c, ring, cross, pl.ds(core_row, 16)], lsem.at[3 + 3 * m]))
        for load in loads:
            load.start()
        stage_loads.append(loads)
    gate_loads = [
        pltpu.make_async_copy(gate_recur, gr, gsem.at[0]),
        pltpu.make_async_copy(gate_input, gi, gsem.at[1]),
    ]
    for load in gate_loads:
        load.start()

    barrier = pltpu.get_barrier_semaphore()
    peers = [at(dx=1), at(dx=-1)]
    peers += [at(dc=1)]
    peers += [at(dy=k, dc=d) for k in range(1, ny) for d in range(2)]
    peers += [at(dz=k, dc=d) for k in range(1, nz) for d in range(2)]
    peers += [of_sp(nsp), of_sp(psp)]
    for peer in peers:
        pl.semaphore_signal(barrier, inc=1, device_id=peer, device_id_type=MESH)
    pl.semaphore_wait(barrier, len(peers))

    own_tok.wait()
    lo, hi = pl.ds(0, half), pl.ds(half, half)
    tok_a_r = remote(tok.at[x, lo], tok.at[x, lo], tsend.at[0], trecv.at[0], at(dx=1))
    tok_b_r = remote(tok.at[x, hi], tok.at[x, hi], tsend.at[1], trecv.at[1], at(dx=1))
    tok_b_l = remote(tok.at[x, hi], tok.at[x, hi], tsend.at[2], trecv.at[2], at(dx=-1))
    tok_a_l = remote(tok.at[x, lo], tok.at[x, lo], tsend.at[3], trecv.at[3], at(dx=-1))
    rel_a = remote(tok.at[left, lo], tok.at[left, lo], tsend.at[4], trecv.at[4], at(dx=1))
    rel_b = remote(tok.at[right, hi], tok.at[right, hi], tsend.at[5], trecv.at[5], at(dx=-1))
    for copy in (tok_a_r, tok_b_l, tok_b_r, tok_a_l):
        copy.start()

    def first_phase(m):
        for load in stage_loads[m]:
            load.wait()
        for k in range(1, ny):
            remote(stage.at[m, 0], wb.at[m, 0, z, y, pl.ds(core_row, 16)], p1send.at[m], p1recv.at[m],
                   at(dy=k, core=0)).start()
        for k in range(1, nz):
            remote(stage.at[m, 1], wb.at[m, 1, y, z, pl.ds(core_row, 16)], p1send.at[m], p1recv.at[m],
                   at(dz=k, core=1)).start()
        other = 1 - c
        r2 = z * c + y * (1 - c)
        q2 = y * c + z * (1 - c)
        remote(stage.at[m, other], wb.at[m, other, r2, q2, pl.ds(core_row, 16)], p1send.at[m], p1recv.at[m],
               at(dc=1)).start()

    def first_phase_done(m):
        pltpu.make_async_copy(dummy, dummy, p1recv.at[m]).wait()

    def ring_at(step):
        return {
            "sp_0": lax.rem(z + (1 - c) * step + nr, nr) * (1 - c) + z * c,
            "sp_1": lax.rem(y + c * step + nr, nr) * c + y * (1 - c),
            "sp_2": c, "tp": x,
        }

    last = nr // 2 - 1
    nq = wb.shape[3]

    def piece(step, way):
        if step < last:
            return pl.ds(0, nq)
        return pl.ds(0, nq // 2) if way == 0 else pl.ds(nq // 2, nq // 2)

    def ring_copy(m, way, step):
        sign = 1 if way == 0 else -1
        block = lax.rem(ring - sign * step + nr, nr)
        ref = wb.at[m, c, block, piece(step, way)]
        return remote(ref, ref, rsend.at[m, way, step], rrecv.at[m, way, step], ring_at(sign))

    def share(m, block, part):
        ref = wb.at[m, c, block, part]
        remote(ref, ref, dsend.at[m], drecv.at[m], at(dc=1)).start()

    def ring_first(m):
        first_phase_done(m)
        for way in range(2):
            ring_copy(m, way, 0).start()
        share(m, ring, pl.ds(0, nq))

    def ring_arrived(m, way, step):
        sign = 1 if way == 0 else -1
        ring_copy(m, way, step).wait_recv()
        if step < last:
            ring_copy(m, way, step + 1).start()
        share(m, lax.rem(ring - sign * (step + 1) + nr, nr), piece(step, way))

    def ring_step(m, step):
        for way in range(2):
            ring_arrived(m, way, step)

    def shared_done(m):
        whole = wb.at[m, 1 - c]
        pltpu.make_async_copy(whole, whole, drecv.at[m]).wait()

    def norm_block(b):
        g = gain[...].astype(F32)

        @pl.loop(0, t // 16)
        def _(i):
            r = pl.ds(pl.multiple_of(i * 16, 16), 16)
            v = tok[b, r, :].astype(F32)
            s = lax.rsqrt(jnp.mean(v * v, axis=-1, keepdims=True) + 1e-06)
            nrm[b, r, :] = (v * s * g).astype(BF16)

    def weight(m, p):
        if p == 0:
            return wb[m, 0].reshape(-1, pw)
        return jnp.concatenate([wb[m, 1, :, k].reshape(-1, pw) for k in range(nq)], axis=0)

    first_phase(0)
    first_phase(1)
    norm_block(x)

    for h in range(heads):
        for k in range(rows // LANES):
            line = decay_shift[h:h + 1, k * LANES:(k + 1) * LANES]
            shiftc[h, k * LANES:(k + 1) * LANES, :] = jnp.transpose(jnp.broadcast_to(line, (LANES, LANES)))
    v = jnp.exp(-decay_param[...])
    rate = v * (1.0 - v * (1 / 2 - v * (1 / 3 - v * (1 / 4 - v * (1 / 5)))))
    rate8 = -8.0 * rate

    ring_first(0)
    ring_first(1)
    first_phase(2)
    for step in range(last):
        ring_step(0, step)
        if step == 0:
            tok_a_r.wait_recv()
            rel_a.start()
            tok_b_l.wait_recv()
            rel_b.start()
        ring_step(1, step)
    ring_step(0, last)
    ring_step(1, last)
    ring_first(2)
    tok_b_r.wait_recv()
    tok_a_l.wait_recv()
    norm_block(left)
    norm_block(right)
    shared_done(0)

    def branch_block(b):
        at_row = pl.ds(pl.multiple_of(8 + b * t, 8), t)
        for p in range(2):
            prod = jnp.dot(nrm[b], weight(0, p), preferred_element_type=F32)
            branch[at_row, p * pw:(p + 1) * pw] = prod.astype(BF16).astype(F32)

    @pl.loop(0, 3)
    def _(k):
        branch_block(lax.rem(x + 3 + k, 4))

    ring_step(2, 0)
    rel_a.wait_recv()
    rel_b.wait_recv()
    norm_block(far)
    branch_block(far)

    tail_copy = remote(branch.at[pl.ds(rows, 8)], tail, xsem.at[0], xsem.at[1], of_sp(nsp))
    tail_copy.start()
    if last >= 1:
        ring_step(2, 1)
    for load in gate_loads:
        load.wait()

    tapf = taps[...].astype(F32)

    def gates(i):
        base = pl.multiple_of(i * t, t)
        win = branch[pl.ds(base, t + 8), :]
        acc = jnp.zeros((t, width), F32)
        for k in range(CONV):
            acc = acc + win[5 + k:5 + k + t] * tapf[k:k + 1]
        conv = acc.astype(BF16)
        at_row = pl.ds(base, t)
        for h in range(heads):
            cols = slice(h * HEAD, (h + 1) * HEAD)
            cb = conv[:, cols]
            cf = cb.astype(F32)
            ur = jnp.dot(cb, gr[h], preferred_element_type=F32)
            ui = jnp.dot(cb, gi[h], preferred_element_type=F32)
            recur = 1.0 / (1.0 + jnp.exp(-ur))
            inlet = 1.0 / (1.0 + jnp.exp(-ui))
            sh = shiftc[h, at_row, :]
            log_decay = recur * rate8[:, cols] + jnp.concatenate([sh] * (HEAD // LANES), axis=1)
            decay = jnp.exp(log_decay)
            u = 2.0 * log_decay
            near = u * (1.0 + u * (1 / 2) * (1.0 + u * (1 / 3) * (1.0 + u * (1 / 4) * (1.0 + u * (1 / 5) * (1.0 + u * (1 / 6))))))
            em1 = jnp.where(u > -0.25, near, decay * decay - 1.0)
            drive = jnp.sqrt(-em1) * inlet * cf
            for g in range(HEAD // LANES):
                lanes = slice(g * LANES, (g + 1) * LANES)
                dec[h * (HEAD // LANES) + g, at_row, :] = decay[:, lanes]
                drv[h * (HEAD // LANES) + g, at_row, :] = drive[:, lanes]

    @pl.loop(0, 3)
    def _(k):
        gates(3 - k)

    tail_copy.wait_recv()
    keep = jnp.where(sp_index > 0, 1.0, 0.0).astype(F32)
    branch[0:8, :] = tail[...] * keep
    gates(0)

    def scan_step(j, carried):
        pos = pl.ds(j, 8, stride=chunk)
        new = []
        for g in range(groups):
            prod, state = carried[g]
            a = dec[g, pos, :]
            b = drv[g, pos, :]
            state = a * state + b
            prod = prod * a
            dec[g, pos, :] = prod
            drv[g, pos, :] = state
            new.append((prod, state))
        return tuple(new)

    one, zero = jnp.ones((8, LANES), F32), jnp.zeros((8, LANES), F32)
    ends = lax.fori_loop(0, chunk, scan_step, ((one, zero),) * groups, unroll=4)
    for g in range(groups):
        prod, state = ends[g]
        pr, st = prod[0:1], state[0:1]
        for i in range(1, 8):
            st = prod[i:i + 1] * st + state[i:i + 1]
            pr = pr * prod[i:i + 1]
        mine1[0:1, g * LANES:(g + 1) * LANES] = pr
        mine1[1:2, g * LANES:(g + 1) * LANES] = st

    me1 = y * 2 + c
    n1 = 2 * ny
    firsts = [at(dc=1)] + [at(dy=k, dc=d) for k in range(1, ny) for d in range(2)]
    for peer in firsts:
        remote(mine1, s1.at[me1], xsem.at[2], xsem.at[3], peer).start()
    s1[me1] = mine1[...]

    def gating_block(b):
        for p in range(2):
            cols = slice(p * pw, (p + 1) * pw)
            prod = jnp.dot(nrm[b], weight(1, p), preferred_element_type=F32)
            v = prod.astype(BF16).astype(F32)
            inner = 0.7978845608028654 * (v + 0.044715 * (v * v * v))
            gel[pl.ds(pl.multiple_of(b * t, t), t), cols] = 0.5 * v * (1.0 + jnp.tanh(inner))

    shared_done(1)

    @pl.loop(0, 2)
    def _(b):
        gating_block(b)

    pltpu.make_async_copy(s1.at[pl.ds(0, n1 - 1)], s1.at[pl.ds(0, n1 - 1)], xsem.at[3]).wait()
    p_all, s_all = s1[0, 0:1], s1[0, 1:2]
    p_in = jnp.where(me1 > 0, p_all, 1.0)
    s_in = jnp.where(me1 > 0, s_all, 0.0)
    for k in range(1, n1):
        s_all = s1[k, 0:1] * s_all + s1[k, 1:2]
        p_all = p_all * s1[k, 0:1]
        p_in = jnp.where(k < me1, p_all, p_in)
        s_in = jnp.where(k < me1, s_all, s_in)
    mine2[0:1, :] = p_all
    mine2[1:2, :] = s_all
    for k in range(1, nz):
        remote(mine2, s2.at[z], xsem.at[4], xsem.at[5], at(dz=k)).start()
    s2[z] = mine2[...]

    @pl.loop(2, 4)
    def _(b):
        gating_block(b)

    for step in range(2, last + 1):
        ring_step(2, step)
    shared_done(2)

    pltpu.make_async_copy(s2.at[pl.ds(0, nz - 1)], s2.at[pl.ds(0, nz - 1)], xsem.at[5]).wait()
    s_plane = jnp.zeros((1, width), F32)
    for k in range(nz - 1):
        s_plane = jnp.where(k < z, s2[k, 0:1] * s_plane + s2[k, 1:2], s_plane)
    carry = p_in * s_plane + s_in
    for g in range(groups):
        lanes = slice(g * LANES, (g + 1) * LANES)
        prod, state = ends[g]
        now = carry[:, lanes]
        for i in range(8):
            cin[g, i:i + 1, :] = now
            now = prod[i:i + 1] * now + state[i:i + 1]

    nt = wb.shape[2]
    tile = wb.shape[3] * wb.shape[4]

    def partial_out(b, emit):
        for i in range(t // chunk):
            r = pl.ds(pl.multiple_of(b * t + i * chunk, chunk), chunk)
            at_chunk = b * (t // chunk) + i
            for g in range(groups):
                lanes = slice(g * LANES, (g + 1) * LANES)
                st = drv[g, r, :] + dec[g, r, :] * cin[g, pl.ds(at_chunk, 1), :]
                mx[i * chunk:(i + 1) * chunk, lanes] = (st * gel[r, lanes]).astype(BF16)

        nt_dims = (((1,), (1,)), ((), ()))

        @pl.loop(0, nz)
        def _(n):
            w0 = wb[2, 0, n].reshape(tile, pw)
            w1 = wb[2, 1, :, n].reshape(tile, pw)
            r = lax.dot_general(mx[:, :pw], w0, nt_dims, preferred_element_type=F32)
            r = r + lax.dot_general(mx[:, pw:], w1, nt_dims, preferred_element_type=F32)
            emit(pl.ds(pl.multiple_of(n * tile, tile), tile), r)

    def emit_to(ref):
        def emit(cols, r):
            ref[:, cols] = r.astype(BF16)
        return emit

    partial_out(far, emit_to(po_far))
    far_a = remote(po_far.at[lo], in_rel.at[0], osend.at[0], orecv.at[0], at(dx=1))
    far_b = remote(po_far.at[hi], in_rel.at[1], osend.at[1], orecv.at[1], at(dx=-1))
    far_a.start()
    far_b.start()
    partial_out(right, emit_to(po_next))
    next_b = remote(po_next.at[hi], in_prev.at[hi], osend.at[2], orecv.at[2], at(dx=1))
    next_b.start()
    partial_out(left, emit_to(po_prev))
    prev_a = remote(po_prev.at[lo], in_next.at[lo], osend.at[3], orecv.at[3], at(dx=-1))
    prev_a.start()

    def emit_own(cols, r):
        outv[:, cols] = r.astype(BF16)

    partial_out(x, emit_own)

    def add_into(ref, base, other):
        @pl.loop(0, half // 16)
        def _(i):
            r = pl.ds(pl.multiple_of(base + i * 16, 16), 16)
            o = pl.ds(pl.multiple_of(i * 16, 16), 16)
            ref[r, :] = (ref[r, :].astype(F32) + other[o, :].astype(F32)).astype(BF16)

    far_a.wait_recv()
    add_into(po_next, 0, in_rel.at[0])
    next_a = remote(po_next.at[lo], in_prev.at[lo], osend.at[4], orecv.at[4], at(dx=1))
    next_a.start()
    far_b.wait_recv()
    add_into(po_prev, half, in_rel.at[1])
    prev_b = remote(po_prev.at[hi], in_next.at[hi], osend.at[5], orecv.at[5], at(dx=-1))
    prev_b.start()

    def finish(base):
        @pl.loop(0, half // 16)
        def _(i):
            r = pl.ds(pl.multiple_of(base + i * 16, 16), 16)
            total = outv[r, :].astype(F32) + in_prev[r, :].astype(F32) + in_next[r, :].astype(F32)
            outv[r, :] = total.astype(BF16)

    next_b.wait_recv()
    prev_a.wait_recv()
    next_a.wait_recv()
    finish(0)
    out_a = pltpu.make_async_copy(outv.at[lo], out.at[lo], lsem.at[0])
    out_a.start()
    prev_b.wait_recv()
    finish(half)
    out_b = pltpu.make_async_copy(outv.at[hi], out.at[hi], lsem.at[1])
    out_b.start()

    for copy in (tok_a_r, tok_b_r, tok_b_l, tok_a_l, rel_a, rel_b, tail_copy, far_a, far_b, next_a, next_b, prev_a, prev_b):
        copy.wait_send()
    for m in range(3):
        pltpu.make_async_copy(dummy, dummy, p1send.at[m]).wait()
        for way in range(2):
            for step in range(last + 1):
                ring_copy(m, way, step).wait_send()
        whole = wb.at[m, c]
        pltpu.make_async_copy(whole, whole, dsend.at[m]).wait()
    pltpu.make_async_copy(s1.at[pl.ds(0, n1 - 1)], s1.at[pl.ds(0, n1 - 1)], xsem.at[2]).wait()
    pltpu.make_async_copy(s2.at[pl.ds(0, nz - 1)], s2.at[pl.ds(0, nz - 1)], xsem.at[4]).wait()
    out_a.wait()
    out_b.wait()


def on_device(
    nz, ny,
    tokens, norm_gain, proj_x, gate_projection, conv_taps, gate_recur, gate_input, decay_param, decay_shift, proj_out,
):
    t, d = tokens.shape
    width = proj_x.shape[1]
    pw = width // 2
    groups = width // LANES
    heads = width // HEAD
    rows = 4 * t
    last = nz // 2
    dma = pltpu.SemaphoreType.DMA
    any_ = pl.BlockSpec(memory_space=pl.ANY)
    vmem = pl.BlockSpec(memory_space=pltpu.VMEM)
    scratch = [
        pltpu.VMEM((4, t, d), BF16),
        pltpu.VMEM((4, t, d), BF16),
        pltpu.VMEM((3, 2, 16, pw), BF16),
        pltpu.VMEM((3, 2, nz, ny, 32, pw), BF16),
        pltpu.VMEM(gate_recur.shape, BF16),
        pltpu.VMEM(gate_input.shape, BF16),
        pltpu.VMEM((rows + 8, width), F32),
        pltpu.VMEM((groups, rows, LANES), F32),
        pltpu.VMEM((groups, rows, LANES), F32),
        pltpu.VMEM((heads, rows, LANES), F32),
        pltpu.VMEM((rows, width), F32),
        pltpu.VMEM((t, width), BF16),
        pltpu.VMEM((8, width), F32),
        pltpu.VMEM((2, width), F32),
        pltpu.VMEM((2 * ny, 2, width), F32),
        pltpu.VMEM((2, width), F32),
        pltpu.VMEM((nz, 2, width), F32),
        pltpu.VMEM((groups, 8, LANES), F32),
        pltpu.VMEM(((ny + nz - 1) * 16, pw), BF16),
        pltpu.VMEM((t, d), BF16),
        pltpu.VMEM((t, d), BF16),
        pltpu.VMEM((t, d), BF16),
        pltpu.VMEM((t, d), BF16),
        pltpu.VMEM((2, t // 2, d), BF16),
        pltpu.VMEM((t, d), BF16),
        pltpu.VMEM((t, d), BF16),
        dma((10,)), dma((2,)), dma((6,)), dma((6,)), dma((3,)), dma((3,)),
        dma((3, 2, last)), dma((3, 2, last)), dma((3,)), dma((3,)), dma((6,)), dma((6,)), dma((6,)),
    ]
    return pl.pallas_call(
        functools.partial(body, nz, ny),
        out_shape=jax.ShapeDtypeStruct((t, d), BF16),
        in_specs=[any_, vmem, any_, any_, vmem, any_, any_, vmem, vmem, any_],
        out_specs=any_,
        scratch_shapes=scratch,
        compiler_params=pltpu.CompilerParams(
            collective_id=0, has_side_effects=True, vmem_limit_bytes=60 * 1024 * 1024
        ),
        name="recurrence",
    )(
        tokens, norm_gain.reshape(1, -1), proj_x, gate_projection, conv_taps, gate_recur, gate_input,
        decay_param.reshape(1, -1), decay_shift, jnp.transpose(proj_out),
    )


def build(mesh, nz, ny):
    split = Mesh(mesh.devices.reshape(nz, ny, 2, mesh.shape["tp"]), ("sp_0", "sp_1", "sp_2", "tp"))
    in_specs = (
        P(SP_TP, None),
        P(),
        P(SP, "tp"),
        P(SP, "tp"),
        P(None, "tp"),
        P("tp", None, None),
        P("tp", None, None),
        P("tp"),
        P("tp", SP),
        P("tp", SP),
    )
    out_specs = P(SP_TP, None)
    return jax.shard_map(
        functools.partial(on_device, nz, ny), mesh=split, in_specs=in_specs, out_specs=out_specs, check_vma=False
    )


def solution(mesh):
    return build(mesh, 8, 8)
```

time: 293 us -> 92.8 us (0.32)
  the two profiles are of different devices: /device:TPU:2 before, /device:TPU:1 now
where the time goes in v1:
time: 92.8 us; the launch traced here: 92.6 us
  Pallas kernels  89.4 us (96%)
  local copies, waits for them, and re-layouts  3.17 us (3%)
    pallas_call x1, Pallas kernels, on_device(): pl.pallas_call(functools.partial(body, nz, ny), out_shape=jax.ShapeDtypeS...  89.4 us
    unnamed x1, local copies, waits for them, and re-layouts  1.88 us

profile of v1, /device:TPU:1, one launch (start us, length us, event | category | flops | bytes accessed | tf_op | source)
XLA Modules:
  0.0 92.6 jit_solution(5301481957548631003)
XLA Ops:
  0.0 1.3 %reshape.6.gain = bf16[1,2048]{1,0:T(2,128)(2,1)} reshape(bf16[2048]{0:T(1024)(128)(2,1)} %param.11) | data formatting | bytes 8192 | tf_op jit(solution)/shard_map/reshape | solution.py:512
  1.3 89.4 %recurrence.1 = bf16[128,2048]{1,0:T(8,128)(2,1)} custom-call(bf16[128,2048]{1,0:T(8,128)(2,1)} %tokens.1, bf16[1,2048]{1,0:T(2,128)(2,1)} %reshape.6.gain, bf16[16,512]{1,0:T(8,128)(2,1)} %proj_x.1, bf16[16,512]{1,0:T(8,128)(2,1)} %gate_proj.1, bf16[4,512]{1,0:T(4,128)(2,1)} %taps.1, bf16[2,256,256]{2,1,0:T(8,128)(2,1)} %gate_recur.1, ...), custom_call_target="tpu_custom_call" | custom-call | tf_op jit(solution)/shard_map/recurrence/pallas_call | solution.py:501
  90.7 1.9 %copy.12 = bf16[128,2048]{1,0:T(8,128)(2,1)} copy(bf16[128,2048]{1,0:T(8,128)(2,1)} %recurrence.1) | data formatting | bytes 1048576

commit v2 on v1

v2 whole, which is shorter than its diff:
```python
import functools

import jax
import jax.numpy as jnp
from jax import lax
from jax.experimental import pallas as pl
from jax.experimental.pallas import tpu as pltpu
from jax.sharding import Mesh
from jax.sharding import PartitionSpec as P

HEAD = 256
CONV = 4
SP = ("sp_0", "sp_1", "sp_2")
SP_TP = ("sp_0", "sp_1", "sp_2", "tp")
MESH = pl.DeviceIdType.MESH
F32 = jnp.float32
BF16 = jnp.bfloat16
LANES = 128


def body(
    nz, ny,
    tokens, gain, proj_x, gate_proj, taps, gate_recur, gate_input, decay_param, decay_shift, proj_out,
    out,
    tok, nrm, stage, wb, gr, gi, branch, dec, drv, shiftc, gel, mx, tail,
    mine1, s1, mine2, s2, cin, dummy, outv,
    mixed, relay, acc,
    lsem, gsem, tsend, trecv, p1send, p1recv, rsend, rrecv, dsend, drecv, xsem, osend, orecv, qsend, qrecv,
):
    z, y, c, x = (lax.axis_index(a) for a in SP_TP)
    t = tok.shape[1]
    half = t // 2
    rows = 4 * t
    chunk = rows // 8
    pitch = chunk + 8
    width = 2 * wb.shape[-1]
    groups = width // LANES
    heads = width // HEAD
    pw = width // 2
    nr = wb.shape[2]
    sp_index = (z * ny + y) * 2 + c
    sp_count = nz * ny * 2

    def at(dz=0, dy=0, dc=None, dx=0, core=None):
        cc = c if dc is None else lax.rem(c + dc, 2)
        cc = cc if core is None else core
        return {
            "sp_0": lax.rem(z + dz + nz, nz), "sp_1": lax.rem(y + dy + ny, ny),
            "sp_2": cc, "tp": lax.rem(x + dx + 4, 4),
        }

    def remote(src, dst, send, recv, where):
        return pltpu.make_async_remote_copy(
            src_ref=src, dst_ref=dst, send_sem=send, recv_sem=recv, device_id=where, device_id_type=MESH
        )

    right, left = lax.rem(x + 1, 4), lax.rem(x + 3, 4)
    far = lax.rem(x + 2, 4)

    nsp = lax.rem(sp_index + 1, sp_count)
    psp = lax.rem(sp_index + sp_count - 1, sp_count)

    def of_sp(s):
        return {"sp_0": s // (2 * ny), "sp_1": lax.rem(s // 2, ny), "sp_2": lax.rem(s, 2), "tp": x}

    own_tok = pltpu.make_async_copy(tokens, tok.at[x], lsem.at[0])
    own_tok.start()
    ring = z * (1 - c) + y * c
    cross = y * (1 - c) + z * c
    core_row = pl.multiple_of(c * 16, 16)
    core_col = pl.multiple_of(c * pw, pw)
    stage_loads = []
    for m, src in enumerate((proj_x, gate_proj, proj_out)):
        slot = m if m < 2 else 2 + x
        loads = []
        for p in range(2):
            loads.append(pltpu.make_async_copy(src.at[:, pl.ds(p * pw, pw)], stage.at[slot, p], lsem.at[1 + 3 * m + p]))
        if m < 2:
            loads.append(pltpu.make_async_copy(
                src.at[:, pl.ds(core_col, pw)], wb.at[m, c, ring, cross, pl.ds(core_row, 16)], lsem.at[3 + 3 * m]))
        for load in loads:
            load.start()
        stage_loads.append(loads)
    gate_loads = [
        pltpu.make_async_copy(gate_recur, gr, gsem.at[0]),
        pltpu.make_async_copy(gate_input, gi, gsem.at[1]),
    ]
    for load in gate_loads:
        load.start()

    barrier = pltpu.get_barrier_semaphore()
    peers = [at(dx=1), at(dx=2), at(dx=3)]
    peers += [at(dc=1)]
    peers += [at(dy=k, dc=d) for k in range(1, ny) for d in range(2)]
    peers += [at(dz=k, dc=d) for k in range(1, nz) for d in range(2)]
    peers += [of_sp(nsp), of_sp(psp)]
    for peer in peers:
        pl.semaphore_signal(barrier, inc=1, device_id=peer, device_id_type=MESH)
    pl.semaphore_wait(barrier, len(peers))

    def quarter(k):
        return remote(stage.at[2 + x], stage.at[2 + x], qsend.at[k - 1], qrecv.at[x], at(dx=k))

    def quarters_start():
        for load in stage_loads[2]:
            load.wait()
        for k in range(1, 4):
            quarter(k).start()

    def quarters_done():
        for k in range(1, 4):
            piece_in = stage.at[2 + lax.rem(x + k, 4)]
            pltpu.make_async_copy(piece_in, piece_in, qrecv.at[lax.rem(x + k, 4)]).wait()
        for m in range(2, 6):
            wb[m, c, ring, cross, pl.ds(core_row, 16), :] = stage[m, c]

    def slot(m):
        return m if m < 2 else 2 + lax.rem(x + (0, 3, 1, 2)[m - 2], 4)

    def first_phase(m):
        if m < 2:
            for load in stage_loads[m]:
                load.wait()
        w = slot(m)
        for k in range(1, ny):
            remote(stage.at[w, 0], wb.at[w, 0, z, y, pl.ds(core_row, 16)], p1send.at[m], p1recv.at[m],
                   at(dy=k, core=0)).start()
        for k in range(1, nz):
            remote(stage.at[w, 1], wb.at[w, 1, y, z, pl.ds(core_row, 16)], p1send.at[m], p1recv.at[m],
                   at(dz=k, core=1)).start()
        other = 1 - c
        r2 = z * c + y * (1 - c)
        q2 = y * c + z * (1 - c)
        remote(stage.at[w, other], wb.at[w, other, r2, q2, pl.ds(core_row, 16)], p1send.at[m], p1recv.at[m],
               at(dc=1)).start()

    def ring_at(step):
        return {
            "sp_0": lax.rem(z + (1 - c) * step + nr, nr) * (1 - c) + z * c,
            "sp_1": lax.rem(y + c * step + nr, nr) * c + y * (1 - c),
            "sp_2": c, "tp": x,
        }

    last = nr // 2 - 1
    nq = wb.shape[3]

    def ring_copy(m, way, step, part):
        sign = 1 if way == 0 else -1
        block = lax.rem(ring - sign * step + nr, nr)
        ref = wb.at[slot(m), c, block, pl.ds(part * (nq // 2), nq // 2)]
        return remote(ref, ref, rsend.at[m, way, step, part], rrecv.at[m, way, step, part], ring_at(sign))

    def parts(way, step):
        return (way, 1 - way) if step < last else (way,)

    def share(m, block, part):
        ref = wb.at[slot(m), c, block, pl.ds(part * (nq // 2), nq // 2)]
        remote(ref, ref, dsend.at[m], drecv.at[m], at(dc=1)).start()

    def ring_first(m):
        pltpu.make_async_copy(dummy, dummy, p1recv.at[m]).wait()
        for k in range(2):
            for way in range(2):
                ring_copy(m, way, 0, parts(way, 0)[k]).start()
        for k in range(2):
            share(m, ring, k)

    def ring_step(m, step):
        for k in range(len(parts(0, step))):
            for way in range(2):
                part = parts(way, step)[k]
                ring_copy(m, way, step, part).wait_recv()
                if step < last and part in parts(way, step + 1):
                    ring_copy(m, way, step + 1, part).start()
                sign = 1 if way == 0 else -1
                share(m, lax.rem(ring - sign * (step + 1) + nr, nr), part)

    def shared_done(m):
        whole = wb.at[slot(m), 1 - c]
        pltpu.make_async_copy(whole, whole, drecv.at[m]).wait()

    gain_rows = gain[...].astype(F32)
    gain_row = jnp.concatenate([gain_rows[k:k + 1] for k in range(gain_rows.shape[0])], axis=1)

    def norm_part(b, base, count):
        g = gain_row

        @pl.loop(0, count // 32)
        def _(i):
            r = pl.ds(pl.multiple_of(base + i * 32, 32), 32)
            v = tok[b, r, :].astype(F32)
            s = lax.rsqrt(jnp.mean(v * v, axis=-1, keepdims=True) + 1e-06)
            nrm[b, r, :] = (v * s * g).astype(BF16)

    def weight(m, p):
        if p == 0:
            return wb[m, 0].reshape(-1, pw)
        return jnp.concatenate([wb[m, 1, :, k].reshape(-1, pw) for k in range(nq)], axis=0)

    quarters_start()
    own_tok.wait()
    lo, hi = pl.ds(0, half), pl.ds(half, half)
    tok_a_r = remote(tok.at[x, lo], tok.at[x, lo], tsend.at[0], trecv.at[0], at(dx=1))
    tok_b_r = remote(tok.at[x, hi], tok.at[x, hi], tsend.at[1], trecv.at[1], at(dx=1))
    tok_b_l = remote(tok.at[x, hi], tok.at[x, hi], tsend.at[2], trecv.at[2], at(dx=-1))
    tok_a_l = remote(tok.at[x, lo], tok.at[x, lo], tsend.at[3], trecv.at[3], at(dx=-1))
    rel_a = remote(tok.at[left, lo], tok.at[left, lo], tsend.at[4], trecv.at[4], at(dx=1))
    rel_b = remote(tok.at[right, hi], tok.at[right, hi], tsend.at[5], trecv.at[5], at(dx=-1))
    for copy in (tok_a_r, tok_b_l, tok_b_r, tok_a_l):
        copy.start()

    first_phase(0)
    first_phase(1)
    norm_part(x, 0, t)

    for h in range(heads):
        for k in range(rows // LANES):
            line = decay_shift[h:h + 1, k * LANES:(k + 1) * LANES]
            shiftc[h, k * LANES:(k + 1) * LANES, :] = jnp.transpose(jnp.broadcast_to(line, (LANES, LANES)))
    v = jnp.exp(-decay_param[...])
    rate = v * (1.0 - v * (1 / 2 - v * (1 / 3 - v * (1 / 4 - v * (1 / 5)))))
    rate8 = -8.0 * rate

    queue = [
        (2, 0), (3, 0), (2, 1), (3, 1), (2, 2), (3, 2), (2, 3), (3, 3), (4, 0), (5, 0),
        (2, 4), (3, 4), (4, 1), (5, 1), (4, 2), (5, 2), (4, 3), (5, 3), (4, 4), (5, 4),
    ]
    queue = [(m, k) for m, k in queue if k <= last + 1]

    def pump(count):
        for _ in range(min(count, len(queue))):
            m, k = queue.pop(0)
            if k == 0:
                ring_first(m)
            else:
                ring_step(m, k - 1)

    ring_first(0)
    ring_first(1)
    quarters_done()
    first_phase(2)
    first_phase(3)
    for step in range(last):
        ring_step(0, step)
        ring_step(1, step)
        if step == 0:
            tok_a_r.wait_recv()
            rel_a.start()
            tok_b_l.wait_recv()
            rel_b.start()
        elif step == 1:
            first_phase(4)
            first_phase(5)
            norm_part(left, 0, half)
            norm_part(right, half, half)
    ring_step(0, last)
    ring_step(1, last)
    pump(2)
    tok_b_r.wait_recv()
    tok_a_l.wait_recv()
    norm_part(left, half, half)
    norm_part(right, 0, half)
    shared_done(0)

    def branch_block(b):
        at_row = pl.ds(pl.multiple_of(8 + b * t, 8), t)
        for p in range(2):
            prod = jnp.dot(nrm[b], weight(0, p), preferred_element_type=F32)
            branch[at_row, p * pw:(p + 1) * pw] = prod.astype(BF16).astype(F32)

    @pl.loop(0, 3)
    def _(k):
        branch_block(lax.rem(x + 3 + k, 4))

    pump(2)
    rel_a.wait_recv()
    rel_b.wait_recv()
    norm_part(far, 0, t)
    branch_block(far)

    tail_copy = remote(branch.at[pl.ds(rows, 8)], tail, xsem.at[0], xsem.at[1], of_sp(nsp))
    tail_copy.start()
    for load in gate_loads:
        load.wait()

    tapf = taps[...].astype(F32)

    def gates(i):
        base = pl.multiple_of(i * t, t)
        win = branch[pl.ds(base, t + 8), :]
        acc = jnp.zeros((t, width), F32)
        for k in range(CONV):
            acc = acc + win[5 + k:5 + k + t] * tapf[k:k + 1]
        conv = acc.astype(BF16)
        at_row = pl.ds(base, t)
        for h in range(heads):
            cols = slice(h * HEAD, (h + 1) * HEAD)
            cb = conv[:, cols]
            cf = cb.astype(F32)
            ur = jnp.dot(cb, gr[h], preferred_element_type=F32)
            ui = jnp.dot(cb, gi[h], preferred_element_type=F32)
            recur = 1.0 / (1.0 + jnp.exp(-ur))
            inlet = 1.0 / (1.0 + jnp.exp(-ui))
            sh = shiftc[h, at_row, :]
            log_decay = recur * rate8[:, cols] + jnp.concatenate([sh] * (HEAD // LANES), axis=1)
            decay = jnp.exp(log_decay)
            u = 2.0 * log_decay
            near = u * (1.0 + u * (1 / 2) * (1.0 + u * (1 / 3) * (1.0 + u * (1 / 4) * (1.0 + u * (1 / 5) * (1.0 + u * (1 / 6))))))
            em1 = jnp.where(u > -0.25, near, decay * decay - 1.0)
            drive = jnp.sqrt(-em1) * inlet * cf
            for g in range(HEAD // LANES):
                lanes = slice(g * LANES, (g + 1) * LANES)
                for k in range(t // chunk):
                    part = slice(k * chunk, (k + 1) * chunk)
                    to = pl.ds(pl.multiple_of((i * (t // chunk) + k) * pitch, 8), chunk)
                    dec[h * (HEAD // LANES) + g, to, :] = decay[part, lanes]
                    drv[h * (HEAD // LANES) + g, to, :] = drive[part, lanes]

    @pl.loop(0, 3)
    def _(k):
        gates(3 - k)

    pump(2)

    tail_copy.wait_recv()
    keep = jnp.where(sp_index > 0, 1.0, 0.0).astype(F32)
    branch[0:8, :] = tail[...] * keep
    gates(0)

    def scan_step(j, carried):
        pos = pl.ds(j, 8, stride=pitch)
        new = []
        for g in range(groups):
            prod, state = carried[g]
            a = dec[g, pos, :]
            b = drv[g, pos, :]
            state = a * state + b
            prod = prod * a
            dec[g, pos, :] = prod
            drv[g, pos, :] = state
            new.append((prod, state))
        return tuple(new)

    one, zero = jnp.ones((8, LANES), F32), jnp.zeros((8, LANES), F32)
    ends = lax.fori_loop(0, chunk, scan_step, ((one, zero),) * groups, unroll=4)
    for g in range(groups):
        prod, state = ends[g]
        pr, st = prod[0:1], state[0:1]
        for i in range(1, 8):
            st = prod[i:i + 1] * st + state[i:i + 1]
            pr = pr * prod[i:i + 1]
        mine1[0:1, g * LANES:(g + 1) * LANES] = pr
        mine1[1:2, g * LANES:(g + 1) * LANES] = st

    me1 = y * 2 + c
    n1 = 2 * ny
    firsts = [at(dc=1)] + [at(dy=k, dc=d) for k in range(1, ny) for d in range(2)]
    for peer in firsts:
        remote(mine1, s1.at[me1], xsem.at[2], xsem.at[3], peer).start()
    s1[me1] = mine1[...]

    def gating_block(b):
        for p in range(2):
            cols = slice(p * pw, (p + 1) * pw)
            prod = jnp.dot(nrm[b], weight(1, p), preferred_element_type=F32)
            v = prod.astype(BF16).astype(F32)
            inner = 0.7978845608028654 * (v + 0.044715 * (v * v * v))
            gel[pl.ds(pl.multiple_of(b * t, t), t), cols] = 0.5 * v * (1.0 + jnp.tanh(inner))

    pump(4)
    shared_done(1)

    @pl.loop(0, 2)
    def _(b):
        gating_block(b)

    pump(2)
    pltpu.make_async_copy(s1.at[pl.ds(0, n1 - 1)], s1.at[pl.ds(0, n1 - 1)], xsem.at[3]).wait()
    p_all, s_all = s1[0, 0:1], s1[0, 1:2]
    p_in = jnp.where(me1 > 0, p_all, 1.0)
    s_in = jnp.where(me1 > 0, s_all, 0.0)
    for k in range(1, n1):
        s_all = s1[k, 0:1] * s_all + s1[k, 1:2]
        p_all = p_all * s1[k, 0:1]
        p_in = jnp.where(k < me1, p_all, p_in)
        s_in = jnp.where(k < me1, s_all, s_in)
    mine2[0:1, :] = p_all
    mine2[1:2, :] = s_all
    for k in range(1, nz):
        remote(mine2, s2.at[z], xsem.at[4], xsem.at[5], at(dz=k)).start()
    s2[z] = mine2[...]

    @pl.loop(2, 4)
    def _(b):
        gating_block(b)

    pump(4)
    pltpu.make_async_copy(s2.at[pl.ds(0, nz - 1)], s2.at[pl.ds(0, nz - 1)], xsem.at[5]).wait()
    s_plane = jnp.zeros((1, width), F32)
    for k in range(nz - 1):
        s_plane = jnp.where(k < z, s2[k, 0:1] * s_plane + s2[k, 1:2], s_plane)
    carry = p_in * s_plane + s_in
    for g in range(groups):
        lanes = slice(g * LANES, (g + 1) * LANES)
        prod, state = ends[g]
        now = carry[:, lanes]
        for i in range(8):
            cin[g, i:i + 1, :] = now
            now = prod[i:i + 1] * now + state[i:i + 1]

    def mixed_block(b):
        for g in range(groups):
            parts = []
            lanes = slice(g * LANES, (g + 1) * LANES)
            for i in range(t // chunk):
                at_chunk = b * (t // chunk) + i
                r = pl.ds(pl.multiple_of(at_chunk * pitch, 8), chunk)
                st = drv[g, r, :] + dec[g, r, :] * cin[g, pl.ds(at_chunk, 1), :]
                parts.append(st * gel[pl.ds(pl.multiple_of(at_chunk * chunk, chunk), chunk), lanes])
            mx[b, lanes, :] = jnp.transpose(jnp.concatenate(parts, axis=0)).astype(BF16)

    half_w = width // 2
    wlo, whi = pl.ds(0, half_w), pl.ds(half_w, half_w)
    mixed_block(far)
    far_a = remote(mx.at[far, wlo], relay.at[0], osend.at[0], orecv.at[0], at(dx=1))
    far_b = remote(mx.at[far, whi], relay.at[1], osend.at[1], orecv.at[1], at(dx=-1))
    far_a.start()
    far_b.start()
    mixed_block(right)
    to_right = remote(mx.at[right], mixed.at[x], osend.at[2], orecv.at[2], at(dx=1))
    to_right.start()
    mixed_block(left)
    to_left = remote(mx.at[left], mixed.at[x], osend.at[3], orecv.at[3], at(dx=-1))
    to_left.start()
    mixed_block(x)
    pump(2)
    far_a.wait_recv()
    pass_a = remote(relay.at[0], mixed.at[left, wlo], osend.at[4], orecv.at[4], at(dx=1))
    pass_a.start()
    far_b.wait_recv()
    pass_b = remote(relay.at[1], mixed.at[right, whi], osend.at[5], orecv.at[5], at(dx=-1))
    pass_b.start()
    tile = ny * 32

    def out_tile(m, source, n):
        w0 = wb[slot(m), 0, n].reshape(tile, pw)
        w1 = wb[slot(m), 1, :, n].reshape(tile, pw)
        r = jnp.dot(w0, source[:pw, :], preferred_element_type=F32)
        return r + jnp.dot(w1, source[pw:, :], preferred_element_type=F32)

    shared_done(2)
    @pl.loop(0, nz, unroll=4)
    def _(n):
        acc[n] = out_tile(2, mx[x], n)

    pump(len(queue))
    shared_done(3)
    shared_done(4)
    to_right.wait_recv()
    to_left.wait_recv()

    @pl.loop(0, nz, unroll=4)
    def _(n):
        acc[n] = acc[n] + out_tile(3, mixed[left], n) + out_tile(4, mixed[right], n)

    shared_done(5)
    pass_a.wait_recv()
    pass_b.wait_recv()

    @pl.loop(0, nz, unroll=4)
    def _(n):
        total = acc[n] + out_tile(5, mixed[far], n)
        outv[:, pl.ds(pl.multiple_of(n * tile, tile), tile)] = jnp.transpose(total).astype(BF16)

    out_a = pltpu.make_async_copy(outv, out, lsem.at[0])
    out_a.start()

    for copy in (tok_a_r, tok_b_r, tok_b_l, tok_a_l, rel_a, rel_b, tail_copy, far_a, far_b, to_right, to_left, pass_a, pass_b,
                 quarter(1), quarter(2), quarter(3)):
        copy.wait_send()
    for m in range(6):
        pltpu.make_async_copy(dummy, dummy, p1send.at[m]).wait()
        for way in range(2):
            for step in range(last + 1):
                for part in parts(way, step):
                    ring_copy(m, way, step, part).wait_send()
        whole = wb.at[slot(m), c]
        pltpu.make_async_copy(whole, whole, dsend.at[m]).wait()
    pltpu.make_async_copy(s1.at[pl.ds(0, n1 - 1)], s1.at[pl.ds(0, n1 - 1)], xsem.at[2]).wait()
    pltpu.make_async_copy(s2.at[pl.ds(0, nz - 1)], s2.at[pl.ds(0, nz - 1)], xsem.at[4]).wait()
    out_a.wait()


def on_device(
    nz, ny,
    tokens, norm_gain, proj_x, gate_projection, conv_taps, gate_recur, gate_input, decay_param, decay_shift, proj_out,
):
    t, d = tokens.shape
    width = proj_x.shape[1]
    pw = width // 2
    groups = width // LANES
    heads = width // HEAD
    rows = 4 * t
    last = nz // 2
    dma = pltpu.SemaphoreType.DMA
    any_ = pl.BlockSpec(memory_space=pl.ANY)
    vmem = pl.BlockSpec(memory_space=pltpu.VMEM)
    scratch = [
        pltpu.VMEM((4, t, d), BF16),
        pltpu.VMEM((4, t, d), BF16),
        pltpu.VMEM((6, 2, 16, pw), BF16),
        pltpu.VMEM((6, 2, nz, ny, 32, pw), BF16),
        pltpu.VMEM(gate_recur.shape, BF16),
        pltpu.VMEM(gate_input.shape, BF16),
        pltpu.VMEM((rows + 8, width), F32),
        pltpu.VMEM((groups, rows + 64, LANES), F32),
        pltpu.VMEM((groups, rows + 64, LANES), F32),
        pltpu.VMEM((heads, rows, LANES), F32),
        pltpu.VMEM((rows, width), F32),
        pltpu.VMEM((4, width, t), BF16),
        pltpu.VMEM((8, width), F32),
        pltpu.VMEM((2, width), F32),
        pltpu.VMEM((2 * ny, 2, width), F32),
        pltpu.VMEM((2, width), F32),
        pltpu.VMEM((nz, 2, width), F32),
        pltpu.VMEM((groups, 8, LANES), F32),
        pltpu.VMEM(((ny + nz - 1) * 16, pw), BF16),
        pltpu.VMEM((t, d), BF16),
        pltpu.VMEM((4, width, t), BF16),
        pltpu.VMEM((2, width // 2, t), BF16),
        pltpu.VMEM((nz, ny * 32, t), F32),
        dma((10,)), dma((2,)), dma((6,)), dma((6,)), dma((6,)), dma((6,)),
        dma((6, 2, last, 2)), dma((6, 2, last, 2)), dma((6,)), dma((6,)), dma((6,)), dma((6,)), dma((6,)), dma((3,)), dma((4,)),
    ]
    return pl.pallas_call(
        functools.partial(body, nz, ny),
        out_shape=jax.ShapeDtypeStruct((t, d), BF16),
        in_specs=[any_, vmem, any_, any_, vmem, any_, any_, vmem, vmem, any_],
        out_specs=any_,
        scratch_shapes=scratch,
        compiler_params=pltpu.CompilerParams(
            collective_id=0, has_side_effects=True, vmem_limit_bytes=60 * 1024 * 1024
        ),
        name="recurrence",
    )(
        tokens, norm_gain.reshape(-1, LANES), proj_x, gate_projection, conv_taps, gate_recur, gate_input,
        decay_param.reshape(1, -1), decay_shift, jnp.transpose(proj_out),
    )


def build(mesh, nz, ny):
    split = Mesh(mesh.devices.reshape(nz, ny, 2, mesh.shape["tp"]), ("sp_0", "sp_1", "sp_2", "tp"))
    in_specs = (
        P(SP_TP, None),
        P(),
        P(SP, "tp"),
        P(SP, "tp"),
        P(None, "tp"),
        P("tp", None, None),
        P("tp", None, None),
        P("tp"),
        P("tp", SP),
        P("tp", SP),
    )
    out_specs = P(SP_TP, None)
    return jax.shard_map(
        functools.partial(on_device, nz, ny), mesh=split, in_specs=in_specs, out_specs=out_specs, check_vma=False
    )


def solution(mesh):
    return build(mesh, 8, 8)
```

time: 92.8 us -> 79.9 us (0.86)
  Pallas kernels: 89.4 us -> 77.8 us
  local copies, waits for them, and re-layouts: 3.17 us -> 1.88 us
    pallas_call x1, Pallas kernels: 89.4 us -> 77.8 us  [on_device(): pl.pallas_call(functools.partial(body, nz, ny), out_shape=jax.ShapeDtypeS...]
    reshape x1 -> x0, local copies, waits for them, and re-layouts: 1.29 us -> none  [on_device(): norm_gain.reshape(1, -1)]
where the time goes in v2:
time: 79.9 us; the launch traced here: 79.7 us
  Pallas kernels  77.8 us (97%)
  local copies, waits for them, and re-layouts  1.88 us (2%)
    pallas_call x1, Pallas kernels, on_device(): pl.pallas_call(functools.partial(body, nz, ny), out_shape=jax.ShapeDtypeS...  77.8 us
    unnamed x1, local copies, waits for them, and re-layouts  1.88 us

profile of v2, /device:TPU:1, one launch (start us, length us, event | category | flops | bytes accessed | tf_op | source)
XLA Modules:
  0.0 79.7 jit_solution(2654081134680060818)
XLA Ops:
  0.0 77.8 %recurrence.1 = bf16[128,2048]{1,0:T(8,128)(2,1)} custom-call(bf16[128,2048]{1,0:T(8,128)(2,1)} %tokens.1, bf16[16,128]{1,0:T(8,128)(2,1)} %bitcast.4, bf16[16,512]{1,0:T(8,128)(2,1)} %proj_x.1, bf16[16,512]{1,0:T(8,128)(2,1)} %gate_proj.1, bf16[4,512]{1,0:T(4,128)(2,1)} %taps.1, bf16[2,256,256]{2,1,0:T(8,128)(2,1)} %gate_recur.1, ...), custom_call_target="tpu_custom_call" | custom-call | tf_op jit(solution)/shard_map/recurrence/pallas_call | solution.py:535
  77.8 1.9 %copy.12 = bf16[128,2048]{1,0:T(8,128)(2,1)} copy(bf16[128,2048]{1,0:T(8,128)(2,1)} %recurrence.1) | data formatting | bytes 1048576

commit v3 on v2

--- a/solution.py
+++ b/solution.py
@@ -15,6 +15,23 @@
 MESH = pl.DeviceIdType.MESH
 F32 = jnp.float32
 BF16 = jnp.bfloat16
+HALVED = (4, 5)
+PLAN = {
+    "start": ("P1",),
+    "r0": ("R10", "Q", "P4", "P5",),
+    "s0": ("R11",),
+    "s1": ("R12", "P2", "P3",),
+    "s2": ("R13", "R40", "R50",),
+    "last": ("R14", "R41", "R51", "R20", "R30",),
+    "far": ("R42", "R52",),
+    "g2": ("R21", "R31",),
+    "scan": ("R43", "R53",),
+    "w1": ("R22", "R32",),
+    "f1": ("R44", "R54",),
+    "w2": ("R23", "R33",),
+    "mix": ("R24", "R34", "S4", "S5",),
+}
+GATING = 2
 LANES = 128
 
 
@@ -25,7 +42,7 @@
     tok, nrm, stage, wb, gr, gi, branch, dec, drv, shiftc, gel, mx, tail,
     mine1, s1, mine2, s2, cin, dummy, outv,
     mixed, relay, acc,
-    lsem, gsem, tsend, trecv, p1send, p1recv, rsend, rrecv, dsend, drecv, xsem, osend, orecv, qsend, qrecv,
+    lsem, gsem, tsend, trecv, p1send, p1recv, rsend, rrecv, dsend, drecv, xsem, osend, orecv, qsend, qrecv, swapsend, swaprecv,
 ):
     z, y, c, x = (lax.axis_index(a) for a in SP_TP)
     t = tok.shape[1]
@@ -112,27 +129,59 @@
             piece_in = stage.at[2 + lax.rem(x + k, 4)]
             pltpu.make_async_copy(piece_in, piece_in, qrecv.at[lax.rem(x + k, 4)]).wait()
         for m in range(2, 6):
-            wb[m, c, ring, cross, pl.ds(core_row, 16), :] = stage[m, c]
-
-    def slot(m):
-        return m if m < 2 else 2 + lax.rem(x + (0, 3, 1, 2)[m - 2], 4)
+            def put(m=m):
+                wb[m, c, ring, cross, pl.ds(core_row, 16), :] = stage[m, c]
+            given(m, cross, put)
+
+    nq = wb.shape[3]
+    hq = nq // 2
+    last = nr // 2 - 1
+    other = 1 - c
+    away_r = z * c + y * (1 - c)
+    away_q = y * c + z * (1 - c)
+
+    def mine(m):
+        return lax.rem(x + m, 2)
+
+    def pieces(m):
+        sends = [
+            (y, [(stage.at[m, 0], wb.at[m, 0, z, y, pl.ds(core_row, 16)], at(dy=k, core=0)) for k in range(1, ny)]),
+            (z, [(stage.at[m, 1], wb.at[m, 1, y, z, pl.ds(core_row, 16)], at(dz=k, core=1)) for k in range(1, nz)]),
+            (away_q, [(stage.at[m, other], wb.at[m, other, away_r, away_q, pl.ds(core_row, 16)], at(dc=1))]),
+        ]
+        return sends
+
+    def given(m, q, act):
+        if m in HALVED:
+            pl.when(q // hq == mine(m))(act)
+        else:
+            act()
 
     def first_phase(m):
         if m < 2:
             for load in stage_loads[m]:
                 load.wait()
-        w = slot(m)
-        for k in range(1, ny):
-            remote(stage.at[w, 0], wb.at[w, 0, z, y, pl.ds(core_row, 16)], p1send.at[m], p1recv.at[m],
-                   at(dy=k, core=0)).start()
-        for k in range(1, nz):
-            remote(stage.at[w, 1], wb.at[w, 1, y, z, pl.ds(core_row, 16)], p1send.at[m], p1recv.at[m],
-                   at(dz=k, core=1)).start()
-        other = 1 - c
-        r2 = z * c + y * (1 - c)
-        q2 = y * c + z * (1 - c)
-        remote(stage.at[w, other], wb.at[w, other, r2, q2, pl.ds(core_row, 16)], p1send.at[m], p1recv.at[m],
-               at(dc=1)).start()
+        for k, (q, sends) in enumerate(pieces(m)):
+            def act(k=k, sends=sends):
+                for src, dst, where in sends:
+                    remote(src, dst, p1send.at[m, k], p1recv.at[m], where).start()
+            given(m, q, act)
+
+    def wait_rows(sem, count):
+        ref = dummy.at[pl.ds(0, 16 * count)]
+        pltpu.make_async_copy(ref, ref, sem).wait()
+
+    def first_phase_done(m):
+        if m in HALVED:
+            own = cross // hq == mine(m)
+            pl.when(own)(lambda: wait_rows(p1recv.at[m], nq - 1))
+            pl.when(jnp.logical_not(own))(lambda: wait_rows(p1recv.at[m], nq))
+        else:
+            wait_rows(p1recv.at[m], 2 * nq - 1)
+
+    def first_phase_sent(m):
+        for k, (q, sends) in enumerate(pieces(m)):
+            given(m, q, lambda k=k, sends=sends: wait_rows(p1send.at[m, k], len(sends)))
 
     def ring_at(step):
         return {
@@ -141,42 +190,74 @@
             "sp_2": c, "tp": x,
         }
 
-    last = nr // 2 - 1
-    nq = wb.shape[3]
+    def half_block(m, block, part):
+        return wb.at[m, c, block, pl.ds(part * hq, hq)]
+
+    def ring_block(way, step):
+        return lax.rem(ring - (1 if way == 0 else -1) * step + nr, nr)
 
     def ring_copy(m, way, step, part):
-        sign = 1 if way == 0 else -1
-        block = lax.rem(ring - sign * step + nr, nr)
-        ref = wb.at[slot(m), c, block, pl.ds(part * (nq // 2), nq // 2)]
-        return remote(ref, ref, rsend.at[m, way, step, part], rrecv.at[m, way, step, part], ring_at(sign))
-
-    def parts(way, step):
+        ref = half_block(m, ring_block(way, step), mine(m) if m in HALVED else part)
+        return remote(ref, ref, rsend.at[m, way, step, part], rrecv.at[m, way, step, part],
+                      ring_at(1 if way == 0 else -1))
+
+    def parts(m, way, step):
+        if m in HALVED:
+            return (0,)
         return (way, 1 - way) if step < last else (way,)
 
+    def turn(m, way, step, act):
+        if m in HALVED and step == last:
+            pl.when(mine(m) == way)(act)
+        else:
+            act()
+
     def share(m, block, part):
-        ref = wb.at[slot(m), c, block, pl.ds(part * (nq // 2), nq // 2)]
+        ref = half_block(m, block, mine(m) if m in HALVED else part)
         remote(ref, ref, dsend.at[m], drecv.at[m], at(dc=1)).start()
+        if m in HALVED:
+            remote(ref, ref, swapsend.at[m], swaprecv.at[m], at(dx=1 - 2 * (block // (nr // 2)))).start()
 
     def ring_first(m):
-        pltpu.make_async_copy(dummy, dummy, p1recv.at[m]).wait()
-        for k in range(2):
+        first_phase_done(m)
+        for k in range(len(parts(m, 0, 0))):
             for way in range(2):
-                ring_copy(m, way, 0, parts(way, 0)[k]).start()
-        for k in range(2):
-            share(m, ring, k)
+                ring_copy(m, way, 0, parts(m, way, 0)[k]).start()
+        for part in sorted(parts(m, 0, 0)):
+            share(m, ring, part)
 
     def ring_step(m, step):
-        for k in range(len(parts(0, step))):
+        for k in range(len(parts(m, 0, step))):
             for way in range(2):
-                part = parts(way, step)[k]
-                ring_copy(m, way, step, part).wait_recv()
-                if step < last and part in parts(way, step + 1):
-                    ring_copy(m, way, step + 1, part).start()
-                sign = 1 if way == 0 else -1
-                share(m, lax.rem(ring - sign * (step + 1) + nr, nr), part)
+                part = parts(m, way, step)[k]
+
+                def act(way=way, part=part):
+                    ring_copy(m, way, step, part).wait_recv()
+                    if step < last and part in parts(m, way, step + 1):
+                        turn(m, way, step + 1, lambda: ring_copy(m, way, step + 1, part).start())
+                    share(m, ring_block(way, step + 1), part)
+
+                turn(m, way, step, act)
+
+    def ring_sent(m):
+        for way in range(2):
+            for step in range(last + 1):
+                for part in parts(m, way, step):
+                    turn(m, way, step, lambda: ring_copy(m, way, step, part).wait_send())
+        if m in HALVED:
+            ref = wb.at[m, c, :, pl.ds(0, hq)]
+            pltpu.make_async_copy(ref, ref, swapsend.at[m]).wait()
+        whole = wb.at[m, c]
+        pltpu.make_async_copy(whole, whole, dsend.at[m]).wait()
+
+    def swapped(m):
+        if m in HALVED:
+            ref = wb.at[m, c, :, pl.ds((1 - mine(m)) * hq, hq)]
+            pltpu.make_async_copy(ref, ref, swaprecv.at[m]).wait()
+            remote(ref, ref, dsend.at[m], drecv.at[m], at(dc=1)).start()
 
     def shared_done(m):
-        whole = wb.at[slot(m), 1 - c]
+        whole = wb.at[m, 1 - c]
         pltpu.make_async_copy(whole, whole, drecv.at[m]).wait()
 
     gain_rows = gain[...].astype(F32)
@@ -196,6 +277,20 @@
         if p == 0:
             return wb[m, 0].reshape(-1, pw)
         return jnp.concatenate([wb[m, 1, :, k].reshape(-1, pw) for k in range(nq)], axis=0)
+
+    def carry_on(place):
+        for op in PLAN.get(place, ()):
+            m = int(op[1:2] or 0)
+            if op[0] == "P":
+                first_phase(m)
+            elif op[0] == "Q":
+                quarters_done()
+            elif op[0] == "S":
+                swapped(m)
+            elif op[2] == "0":
+                ring_first(m)
+            else:
+                ring_step(m, int(op[2]) - 1)
 
     quarters_start()
     own_tok.wait()
@@ -210,7 +305,7 @@
         copy.start()
 
     first_phase(0)
-    first_phase(1)
+    carry_on("start")
     norm_part(x, 0, t)
 
     for h in range(heads):
@@ -221,45 +316,29 @@
     rate = v * (1.0 - v * (1 / 2 - v * (1 / 3 - v * (1 / 4 - v * (1 / 5)))))
     rate8 = -8.0 * rate
 
-    queue = [
-        (2, 0), (3, 0), (2, 1), (3, 1), (2, 2), (3, 2), (2, 3), (3, 3), (4, 0), (5, 0),
-        (2, 4), (3, 4), (4, 1), (5, 1), (4, 2), (5, 2), (4, 3), (5, 3), (4, 4), (5, 4),
-    ]
-    queue = [(m, k) for m, k in queue if k <= last + 1]
-
-    def pump(count):
-        for _ in range(min(count, len(queue))):
-            m, k = queue.pop(0)
-            if k == 0:
-                ring_first(m)
-            else:
-                ring_step(m, k - 1)
-
     ring_first(0)
-    ring_first(1)
-    quarters_done()
-    first_phase(2)
-    first_phase(3)
-    for step in range(last):
-        ring_step(0, step)
-        ring_step(1, step)
-        if step == 0:
-            tok_a_r.wait_recv()
-            rel_a.start()
-            tok_b_l.wait_recv()
-            rel_b.start()
-        elif step == 1:
-            first_phase(4)
-            first_phase(5)
-            norm_part(left, 0, half)
-            norm_part(right, half, half)
-    ring_step(0, last)
-    ring_step(1, last)
-    pump(2)
+    carry_on("r0")
+    ring_step(0, 0)
+    tok_a_r.wait_recv()
+    rel_a.start()
+    tok_b_l.wait_recv()
+    rel_b.start()
+    carry_on("s0")
+    ring_step(0, 1)
+    carry_on("s1")
+    norm_part(left, 0, half)
+    norm_part(right, half, half)
+    ring_step(0, 2)
+    carry_on("s2")
     tok_b_r.wait_recv()
     tok_a_l.wait_recv()
     norm_part(left, half, half)
     norm_part(right, 0, half)
+    rel_a.wait_recv()
+    rel_b.wait_recv()
+    norm_part(far, 0, t)
+    ring_step(0, last)
+    carry_on("last")
     shared_done(0)
 
     def branch_block(b):
@@ -268,18 +347,15 @@
             prod = jnp.dot(nrm[b], weight(0, p), preferred_element_type=F32)
             branch[at_row, p * pw:(p + 1) * pw] = prod.astype(BF16).astype(F32)
 
-    @pl.loop(0, 3)
-    def _(k):
-        branch_block(lax.rem(x + 3 + k, 4))
-
-    pump(2)
-    rel_a.wait_recv()
-    rel_b.wait_recv()
-    norm_part(far, 0, t)
-    branch_block(far)
+    @pl.loop(0, 4)
+    def _(b):
+        branch_block(b)
+
+    carry_on("branch")
 
     tail_copy = remote(branch.at[pl.ds(rows, 8)], tail, xsem.at[0], xsem.at[1], of_sp(nsp))
     tail_copy.start()
+    carry_on("far")
     for load in gate_loads:
         load.wait()
 
@@ -316,11 +392,12 @@
                     dec[h * (HEAD // LANES) + g, to, :] = decay[part, lanes]
                     drv[h * (HEAD // LANES) + g, to, :] = drive[part, lanes]
 
-    @pl.loop(0, 3)
-    def _(k):
-        gates(3 - k)
-
-    pump(2)
+    gates(3)
+    carry_on("g3")
+    gates(2)
+    carry_on("g2")
+    gates(1)
+    carry_on("g1")
 
     tail_copy.wait_recv()
     keep = jnp.where(sp_index > 0, 1.0, 0.0).astype(F32)
@@ -367,14 +444,17 @@
             inner = 0.7978845608028654 * (v + 0.044715 * (v * v * v))
             gel[pl.ds(pl.multiple_of(b * t, t), t), cols] = 0.5 * v * (1.0 + jnp.tanh(inner))
 
-    pump(4)
-    shared_done(1)
-
-    @pl.loop(0, 2)
-    def _(b):
-        gating_block(b)
-
-    pump(2)
+    def gating(first, end):
+        if end > first:
+            @pl.loop(first, end)
+            def _(b):
+                gating_block(b)
+
+    carry_on("scan")
+    if GATING:
+        shared_done(1)
+        gating(0, GATING)
+    carry_on("w1")
     pltpu.make_async_copy(s1.at[pl.ds(0, n1 - 1)], s1.at[pl.ds(0, n1 - 1)], xsem.at[3]).wait()
     p_all, s_all = s1[0, 0:1], s1[0, 1:2]
     p_in = jnp.where(me1 > 0, p_all, 1.0)
@@ -390,11 +470,11 @@
         remote(mine2, s2.at[z], xsem.at[4], xsem.at[5], at(dz=k)).start()
     s2[z] = mine2[...]
 
-    @pl.loop(2, 4)
-    def _(b):
-        gating_block(b)
-
-    pump(4)
+    carry_on("f1")
+    if not GATING:
+        shared_done(1)
+    gating(GATING, 4)
+    carry_on("w2")
     pltpu.make_async_copy(s2.at[pl.ds(0, nz - 1)], s2.at[pl.ds(0, nz - 1)], xsem.at[5]).wait()
     s_plane = jnp.zeros((1, width), F32)
     for k in range(nz - 1):
@@ -433,62 +513,59 @@
     to_left = remote(mx.at[left], mixed.at[x], osend.at[3], orecv.at[3], at(dx=-1))
     to_left.start()
     mixed_block(x)
-    pump(2)
+    carry_on("mix")
     far_a.wait_recv()
     pass_a = remote(relay.at[0], mixed.at[left, wlo], osend.at[4], orecv.at[4], at(dx=1))
     pass_a.start()
     far_b.wait_recv()
     pass_b = remote(relay.at[1], mixed.at[right, whi], osend.at[5], orecv.at[5], at(dx=-1))
     pass_b.start()
+    carry_on("rel")
+
     tile = ny * 32
 
-    def out_tile(m, source, n):
-        w0 = wb[slot(m), 0, n].reshape(tile, pw)
-        w1 = wb[slot(m), 1, :, n].reshape(tile, pw)
+    def out_tile(q, source, n):
+        w0 = wb[2 + q, 0, n].reshape(tile, pw)
+        w1 = wb[2 + q, 1, :, n].reshape(tile, pw)
         r = jnp.dot(w0, source[:pw, :], preferred_element_type=F32)
         return r + jnp.dot(w1, source[pw:, :], preferred_element_type=F32)
 
-    shared_done(2)
+    for m in range(2, 6):
+        shared_done(m)
     @pl.loop(0, nz, unroll=4)
     def _(n):
-        acc[n] = out_tile(2, mx[x], n)
-
-    pump(len(queue))
-    shared_done(3)
-    shared_done(4)
+        acc[n] = out_tile(x, mx[x], n)
+
     to_right.wait_recv()
     to_left.wait_recv()
 
     @pl.loop(0, nz, unroll=4)
     def _(n):
-        acc[n] = acc[n] + out_tile(3, mixed[left], n) + out_tile(4, mixed[right], n)
-
-    shared_done(5)
+        acc[n] = acc[n] + out_tile(left, mixed[left], n) + out_tile(right, mixed[right], n)
+
     pass_a.wait_recv()
     pass_b.wait_recv()
-
-    @pl.loop(0, nz, unroll=4)
-    def _(n):
-        total = acc[n] + out_tile(5, mixed[far], n)
-        outv[:, pl.ds(pl.multiple_of(n * tile, tile), tile)] = jnp.transpose(total).astype(BF16)
-
-    out_a = pltpu.make_async_copy(outv, out, lsem.at[0])
-    out_a.start()
+    leave = []
+    for k in range(2):
+        @pl.loop(k * (nz // 2), (k + 1) * (nz // 2), unroll=nz // 2)
+        def _(n):
+            total = acc[n] + out_tile(far, mixed[far], n)
+            outv[:, pl.ds(pl.multiple_of(n * tile, tile), tile)] = jnp.transpose(total).astype(BF16)
+
+        side = pl.ds(k * (nz // 2) * tile, (nz // 2) * tile)
+        leave.append(pltpu.make_async_copy(outv.at[:, side], out.at[:, side], lsem.at[k]))
+        leave[k].start()
 
     for copy in (tok_a_r, tok_b_r, tok_b_l, tok_a_l, rel_a, rel_b, tail_copy, far_a, far_b, to_right, to_left, pass_a, pass_b,
                  quarter(1), quarter(2), quarter(3)):
         copy.wait_send()
     for m in range(6):
-        pltpu.make_async_copy(dummy, dummy, p1send.at[m]).wait()
-        for way in range(2):
-            for step in range(last + 1):
-                for part in parts(way, step):
-                    ring_copy(m, way, step, part).wait_send()
-        whole = wb.at[slot(m), c]
-        pltpu.make_async_copy(whole, whole, dsend.at[m]).wait()
+        first_phase_sent(m)
+        ring_sent(m)
     pltpu.make_async_copy(s1.at[pl.ds(0, n1 - 1)], s1.at[pl.ds(0, n1 - 1)], xsem.at[2]).wait()
     pltpu.make_async_copy(s2.at[pl.ds(0, nz - 1)], s2.at[pl.ds(0, nz - 1)], xsem.at[4]).wait()
-    out_a.wait()
+    for copy in leave:
+        copy.wait()
 
 
 def on_device(
@@ -529,8 +606,9 @@
         pltpu.VMEM((4, width, t), BF16),
         pltpu.VMEM((2, width // 2, t), BF16),
         pltpu.VMEM((nz, ny * 32, t), F32),
-        dma((10,)), dma((2,)), dma((6,)), dma((6,)), dma((6,)), dma((6,)),
+        dma((10,)), dma((2,)), dma((6,)), dma((6,)), dma((6, 3)), dma((6,)),
         dma((6, 2, last, 2)), dma((6, 2, last, 2)), dma((6,)), dma((6,)), dma((6,)), dma((6,)), dma((6,)), dma((3,)), dma((4,)),
+        dma((6,)), dma((6,)),
     ]
     return pl.pallas_call(
         functools.partial(body, nz, ny),

time: 79.9 us -> 72.1 us (0.902)
  Pallas kernels: 77.8 us -> 70 us
    pallas_call x1, Pallas kernels: 77.8 us -> 70 us  [on_device(): pl.pallas_call(functools.partial(body, nz, ny), out_shape=jax.ShapeDtypeS...]
where the time goes in v3:
time: 72.1 us; the launch traced here: 71.9 us
  Pallas kernels  70 us (97%)
  local copies, waits for them, and re-layouts  1.88 us (3%)
    pallas_call x1, Pallas kernels, on_device(): pl.pallas_call(functools.partial(body, nz, ny), out_shape=jax.ShapeDtypeS...  70 us
    unnamed x1, local copies, waits for them, and re-layouts  1.88 us

profile of v3, /device:TPU:1, one launch (start us, length us, event | category | flops | bytes accessed | tf_op | source)
XLA Modules:
  0.0 71.9 jit_solution(11185911209501550592)
XLA Ops:
  0.0 70.0 %recurrence.1 = bf16[128,2048]{1,0:T(8,128)(2,1)} custom-call(bf16[128,2048]{1,0:T(8,128)(2,1)} %tokens.1, bf16[16,128]{1,0:T(8,128)(2,1)} %bitcast.4, bf16[16,512]{1,0:T(8,128)(2,1)} %proj_x.1, bf16[16,512]{1,0:T(8,128)(2,1)} %gate_proj.1, bf16[4,512]{1,0:T(4,128)(2,1)} %taps.1, bf16[2,256,256]{2,1,0:T(8,128)(2,1)} %gate_recur.1, ...), custom_call_target="tpu_custom_call" | custom-call | tf_op jit(solution)/shard_map/recurrence/pallas_call | solution.py:613
  70.1 1.9 %copy.12 = bf16[128,2048]{1,0:T(8,128)(2,1)} copy(bf16[128,2048]{1,0:T(8,128)(2,1)} %recurrence.1) | data formatting | bytes 1048576

commit v4 on v3

--- a/solution.py
+++ b/solution.py
@@ -37,11 +37,12 @@
 
 def body(
     nz, ny,
-    tokens, gain, proj_x, gate_proj, taps, gate_recur, gate_input, decay_param, decay_shift, proj_out,
+    tokens, gain_in, proj_x, gate_proj, taps_in, gate_recur, gate_input, param_in, shift_in, proj_out,
     out,
     tok, nrm, stage, wb, gr, gi, branch, dec, drv, shiftc, gel, mx, tail,
     mine1, s1, mine2, s2, cin, dummy, outv,
     mixed, relay, acc,
+    gain, taps, decay_param, decay_shift,
     lsem, gsem, tsend, trecv, p1send, p1recv, rsend, rrecv, dsend, drecv, xsem, osend, orecv, qsend, qrecv, swapsend, swaprecv,
 ):
     z, y, c, x = (lax.axis_index(a) for a in SP_TP)
@@ -101,8 +102,14 @@
     gate_loads = [
         pltpu.make_async_copy(gate_recur, gr, gsem.at[0]),
         pltpu.make_async_copy(gate_input, gi, gsem.at[1]),
+        pltpu.make_async_copy(taps_in, taps, gsem.at[2]),
     ]
-    for load in gate_loads:
+    early_loads = [
+        pltpu.make_async_copy(gain_in, gain, gsem.at[3]),
+        pltpu.make_async_copy(param_in, decay_param, gsem.at[4]),
+        pltpu.make_async_copy(shift_in, decay_shift, gsem.at[5]),
+    ]
+    for load in early_loads + gate_loads:
         load.start()
 
     barrier = pltpu.get_barrier_semaphore()
@@ -259,9 +266,6 @@
     def shared_done(m):
         whole = wb.at[m, 1 - c]
         pltpu.make_async_copy(whole, whole, drecv.at[m]).wait()
-
-    gain_rows = gain[...].astype(F32)
-    gain_row = jnp.concatenate([gain_rows[k:k + 1] for k in range(gain_rows.shape[0])], axis=1)
 
     def norm_part(b, base, count):
         g = gain_row
@@ -306,6 +310,10 @@
 
     first_phase(0)
     carry_on("start")
+    for load in early_loads:
+        load.wait()
+    gain_rows = gain[...].astype(F32)
+    gain_row = jnp.concatenate([gain_rows[k:k + 1] for k in range(gain_rows.shape[0])], axis=1)
     norm_part(x, 0, t)
 
     for h in range(heads):
@@ -581,7 +589,6 @@
     last = nz // 2
     dma = pltpu.SemaphoreType.DMA
     any_ = pl.BlockSpec(memory_space=pl.ANY)
-    vmem = pl.BlockSpec(memory_space=pltpu.VMEM)
     scratch = [
         pltpu.VMEM((4, t, d), BF16),
         pltpu.VMEM((4, t, d), BF16),
@@ -590,8 +597,8 @@
         pltpu.VMEM(gate_recur.shape, BF16),
         pltpu.VMEM(gate_input.shape, BF16),
         pltpu.VMEM((rows + 8, width), F32),
-        pltpu.VMEM((groups, rows + 64, LANES), F32),
-        pltpu.VMEM((groups, rows + 64, LANES), F32),
+        pltpu.VMEM((groups, rows + 136, LANES), F32),
+        pltpu.VMEM((groups, rows + 136, LANES), F32),
         pltpu.VMEM((heads, rows, LANES), F32),
         pltpu.VMEM((rows, width), F32),
         pltpu.VMEM((4, width, t), BF16),
@@ -606,14 +613,18 @@
         pltpu.VMEM((4, width, t), BF16),
         pltpu.VMEM((2, width // 2, t), BF16),
         pltpu.VMEM((nz, ny * 32, t), F32),
-        dma((10,)), dma((2,)), dma((6,)), dma((6,)), dma((6, 3)), dma((6,)),
+        pltpu.VMEM((d // LANES, LANES), BF16),
+        pltpu.VMEM(conv_taps.shape, BF16),
+        pltpu.VMEM((1, width), F32),
+        pltpu.VMEM(decay_shift.shape, F32),
+        dma((10,)), dma((6,)), dma((6,)), dma((6,)), dma((6, 3)), dma((6,)),
         dma((6, 2, last, 2)), dma((6, 2, last, 2)), dma((6,)), dma((6,)), dma((6,)), dma((6,)), dma((6,)), dma((3,)), dma((4,)),
         dma((6,)), dma((6,)),
     ]
     return pl.pallas_call(
         functools.partial(body, nz, ny),
         out_shape=jax.ShapeDtypeStruct((t, d), BF16),
-        in_specs=[any_, vmem, any_, any_, vmem, any_, any_, vmem, vmem, any_],
+        in_specs=[any_] * 10,
         out_specs=any_,
         scratch_shapes=scratch,
         compiler_params=pltpu.CompilerParams(

time: 72.1 us -> 71.6 us (level)
  no operation moved by 1% of the time
where the time goes in v4:
time: 71.6 us; the launch traced here: 71.4 us
  Pallas kernels  69.5 us (97%)
  local copies, waits for them, and re-layouts  1.88 us (3%)
    pallas_call x1, Pallas kernels, on_device(): pl.pallas_call(functools.partial(body, nz, ny), out_shape=jax.ShapeDtypeS...  69.5 us
    unnamed x1, local copies, waits for them, and re-layouts  1.88 us

profile of v4, /device:TPU:1, one launch (start us, length us, event | category | flops | bytes accessed | tf_op | source)
XLA Modules:
  0.0 71.4 jit_solution(5898914494426985185)
XLA Ops:
  0.0 69.5 %recurrence.1 = bf16[128,2048]{1,0:T(8,128)(2,1)} custom-call(bf16[128,2048]{1,0:T(8,128)(2,1)} %tokens.1, bf16[16,128]{1,0:T(8,128)(2,1)} %bitcast.4, bf16[16,512]{1,0:T(8,128)(2,1)} %proj_x.1, bf16[16,512]{1,0:T(8,128)(2,1)} %gate_proj.1, bf16[4,512]{1,0:T(4,128)(2,1)} %taps_in.1, bf16[2,256,256]{2,1,0:T(8,128)(2,1)} %gate_recur.1, ...), custom_call_target="tpu_custom_call" | custom-call | tf_op jit(solution)/shard_map/recurrence/pallas_call | solution.py:624
  69.5 1.9 %copy.12 = bf16[128,2048]{1,0:T(8,128)(2,1)} copy(bf16[128,2048]{1,0:T(8,128)(2,1)} %recurrence.1) | data formatting | bytes 1048576

commit v5 on v4

--- a/solution.py
+++ b/solution.py
@@ -20,14 +20,14 @@
     "start": ("P1",),
     "r0": ("R10", "Q", "P4", "P5",),
     "s0": ("R11",),
-    "s1": ("R12", "P2", "P3",),
-    "s2": ("R13", "R40", "R50",),
-    "last": ("R14", "R41", "R51", "R20", "R30",),
-    "far": ("R42", "R52",),
-    "g2": ("R21", "R31",),
-    "scan": ("R43", "R53",),
-    "w1": ("R22", "R32",),
-    "f1": ("R44", "R54",),
+    "s1": ("R12", "P2",),
+    "s2": ("R13", "R40", "R50", "P3",),
+    "last": ("R14", "R41", "R51", "R20",),
+    "far": ("R42", "R52", "R30",),
+    "g2": ("R21",),
+    "scan": ("R43", "R53", "R31",),
+    "w1": ("R22",),
+    "f1": ("R32", "R44", "R54",),
     "w2": ("R23", "R33",),
     "mix": ("R24", "R34", "S4", "S5",),
 }

time: 71.6 us -> 71.6 us (level)
  no operation moved by 1% of the time
where the time goes in v5:
time: 71.6 us; the launch traced here: 71.4 us
  Pallas kernels  69.6 us (97%)
  local copies, waits for them, and re-layouts  1.88 us (3%)
    pallas_call x1, Pallas kernels, on_device(): pl.pallas_call(functools.partial(body, nz, ny), out_shape=jax.ShapeDtypeS...  69.6 us
    unnamed x1, local copies, waits for them, and re-layouts  1.88 us

profile of v5, /device:TPU:1, one launch (start us, length us, event | category | flops | bytes accessed | tf_op | source)
XLA Modules:
  0.0 71.4 jit_solution(9929442148411750181)
XLA Ops:
  0.0 69.6 %recurrence.1 = bf16[128,2048]{1,0:T(8,128)(2,1)} custom-call(bf16[128,2048]{1,0:T(8,128)(2,1)} %tokens.1, bf16[16,128]{1,0:T(8,128)(2,1)} %bitcast.4, bf16[16,512]{1,0:T(8,128)(2,1)} %proj_x.1, bf16[16,512]{1,0:T(8,128)(2,1)} %gate_proj.1, bf16[4,512]{1,0:T(4,128)(2,1)} %taps_in.1, bf16[2,256,256]{2,1,0:T(8,128)(2,1)} %gate_recur.1, ...), custom_call_target="tpu_custom_call" | custom-call | tf_op jit(solution)/shard_map/recurrence/pallas_call | solution.py:624
  69.6 1.9 %copy.12 = bf16[128,2048]{1,0:T(8,128)(2,1)} copy(bf16[128,2048]{1,0:T(8,128)(2,1)} %recurrence.1) | data formatting | bytes 1048576
